TPU v7x, 128 devices: a whole 4x4x4 slice. The times are simulated.
128 devices in a mesh: sp: 16 (over z, x), tp: 8 (over y, core).
Axes of the slice: x: 4, y: 4, z: 4, core: 2. Of those that a mesh axis runs over, the one named last changes fastest.
Arguments:
- prompt: bfloat16 [4, 8192, 4096], P(None, 'sp'), may hold values from -6 to 6
- key_weight: bfloat16 [4096, 1024], P(None, 'tp'), may hold values from -0.09375 to 0.09375
- value_weight: bfloat16 [4096, 2048], P(None, 'tp'), may hold values from -0.09375 to 0.09375
- input_gate_weight: bfloat16 [4096, 16], P(None, 'tp'), may hold values from -0.09375 to 0.09375
- forget_gate_weight: bfloat16 [4096, 16], P(None, 'tp'), may hold values from -0.09375 to 0.09375
- forget_bias: float32 [16], P('tp'), may hold values from 3 to 11
- key_taps: bfloat16 [3, 1024], P(None, 'tp'), may hold values from -3 to 3
- extra_decay: float32 [4, 8192, 16], P(None, 'sp', 'tp'), may hold values from -1.5 to 0
- new_query: bfloat16 [4, 16, 64], P(None, 'tp'), may hold values from -6 to 6
- new_key: bfloat16 [4, 16, 64], P(None, 'tp'), may hold values from -6 to 6
- new_value: bfloat16 [4, 16, 128], P(None, 'tp', 'sp'), may hold values from -6 to 6
- new_input_gate: float32 [4, 16], P(None, 'tp'), may hold values from 2 to 7
- new_forget_gate: float32 [4, 16], P(None, 'tp'), may hold values from -2 to 4
- out_weight: bfloat16 [16, 128, 4096], P('tp', 'sp'), may hold values from -0.125 to 0.125
Outputs:
- cache_memory: bfloat16 [4, 16, 64, 128], P(None, 'tp', None, 'sp')
- cache_norm: bfloat16 [4, 16, 64], P(None, 'tp', 'sp')
- cache_peak: float32 [4, 16], P(None, 'tp')
- read_out: bfloat16 [4, 4096], P(None, ('sp', 'tp'))
All inputs are finite; a program needn't handle non-finite values.
Results may differ from a plain program's by a relative error of at most 0.012.
The roundings to bfloat16 on the way count: a program that leaves them out, or rounds other values in their place, can miss the bound.
Values may be sent and summed in bfloat16 or wider, within the bound.
No kernel may reach another device: no remote copies, remote signals or barrier semaphores. Data moves between devices by JAX's collectives and lax.ppermute only.
A program may use at most 64 MiB of HBM per device.

v0:
```python
import functools

import jax
import jax.numpy as jnp
from jax import lax
from jax.sharding import Mesh
from jax.sharding import PartitionSpec as P

KEY_DIM = 64
SP = ("sp_0", "sp_1")
SP_TP = ("sp_0", "sp_1", "tp_0", "tp_1")
TP = ("tp_0", "tp_1")


def with_halo(shard, sides, width):
    for axis, dim in sides:
        devices, length = (lax.axis_size(axis), shard.shape[dim])
        up = [(i, (i + 1) % devices) for i in range(devices - 1)]
        down = [(j, i) for i, j in up]
        last = lax.slice_in_dim(shard, length - width, length, axis=dim)
        leading = lax.slice_in_dim(shard, 0, width, axis=dim)
        before = lax.ppermute(last, axis, up)
        after = lax.ppermute(leading, axis, down)
        shard = jnp.concatenate([before, shard, after], axis=dim)
    return shard


def copy_for_each(shard, axis):
    copies = jnp.broadcast_to(shard, (lax.axis_size(axis), *shard.shape))
    return lax.all_to_all(copies, axis, split_axis=0, concat_axis=0, tiled=True)


def joined_by_halves(pieces, combine):
    while len(jax.tree.leaves(pieces)[0]) > 1:
        pieces = jax.vmap(combine)(*(pieces[side::2] for side in (0, 1)))
    return pieces[0]


def prefix(shard, axis, combine, identity):
    devices, here = (lax.axis_size(axis), lax.axis_index(axis))
    passed = jnp.arange(devices) > here

    def kept(part, zero, own):
        part = jnp.where(
            passed.reshape(-1, *(1 for _ in own.shape)), part, jnp.asarray(zero, own.dtype)
        )
        return part[::-1]

    pieces = copy_for_each(shard, axis)
    return joined_by_halves(kept(pieces, identity, shard), combine)


def by_axis(shard, axes):
    return functools.reduce(lax.pmax, axes, shard)


def in_blocks(shard, dim, devices):
    before, after = (shard.shape[:dim], shard.shape[dim + 1 :])
    return jnp.moveaxis(shard.reshape(*before, devices, -1, *after), dim, 0)


def sum_at_owner(shard, axis, dim):
    devices = lax.axis_size(axis)
    parts = lax.all_to_all(in_blocks(shard, dim, devices), axis, 0, 0, tiled=True)
    return jnp.sum(parts, axis=0)


def over_axes(shard, axes):
    for axis in axes:
        shard = lax.psum(shard, axis)
    return shard


def sum_by_axis(shard, axes, dim):
    far, near = axes
    own = sum_at_owner(in_blocks(shard, dim, lax.axis_size(far)), near, dim + 1)
    return jnp.sum(lax.all_to_all(own, far, 0, 0, tiled=True), axis=0)


def widen(rounded):
    return lax.optimization_barrier(rounded).astype(jnp.float32)


def project(seq_rows, key_weight, value_weight, input_gate_weight, forget_gate_weight):
    seq_count, pos_count, width = seq_rows.shape
    flat_rows = seq_rows.reshape(seq_count * pos_count, width)
    key_raw = jnp.dot(flat_rows, key_weight, preferred_element_type=jnp.float32).astype(
        jnp.bfloat16
    )
    values = jnp.dot(flat_rows, value_weight, preferred_element_type=jnp.float32).astype(
        jnp.bfloat16
    )
    gate_weight = jnp.concatenate([input_gate_weight, forget_gate_weight], axis=1)
    gate_pre = jnp.dot(flat_rows, gate_weight, preferred_element_type=jnp.float32).astype(
        jnp.bfloat16
    )
    return (
        key_raw.reshape(seq_count, pos_count, -1),
        values.reshape(seq_count, pos_count, -1),
        gate_pre.reshape(seq_count, pos_count, -1),
    )


def key_conv(padded, key_taps):
    tap_f32 = key_taps.astype(jnp.float32)
    mixed = tap_f32[0] * padded[:, :-2] + tap_f32[1] * padded[:, 1:-1] + tap_f32[2] * padded[:, 2:]
    return (jax.nn.silu(mixed) * KEY_DIM ** (-0.5)).astype(jnp.bfloat16)


def gate_parts(gate_pre, forget_bias, extra):
    head_count = extra.shape[-1]
    gate_f32 = widen(gate_pre)
    input_pre = gate_f32[..., :head_count]
    log_forget = jax.nn.log_sigmoid(gate_f32[..., head_count:] + forget_bias) + extra
    return (input_pre, log_forget)


def suffix_of(log_forget):
    return jnp.sum(log_forget, axis=1, keepdims=True) - jnp.cumsum(log_forget, axis=1)


def add_later(earlier, latter):
    return earlier + latter


def body(
    prompt,
    key_weight,
    value_weight,
    input_gate_weight,
    forget_gate_weight,
    forget_bias,
    key_taps,
    extra_decay,
    new_query,
    new_key,
    new_value,
    new_input_gate,
    new_forget_gate,
    out_weight,
):
    seq_count = prompt.shape[0]
    head_count = extra_decay.shape[-1]
    key_size = new_key.shape[2]
    sp_count = lax.axis_size(SP)
    sp_index = lax.axis_index(SP)
    key_cols = key_size // sp_count
    key_raw, values, gate_pre = project(
        prompt, key_weight, value_weight, input_gate_weight, forget_gate_weight
    )
    input_pre, log_forget = gate_parts(gate_pre, forget_bias, extra_decay)
    padded = with_halo(key_raw, ((SP, 1),), 1)
    key_rows = key_conv(padded, key_taps)
    seg_total = jnp.sum(log_forget, axis=1)
    later_sum = prefix(seg_total, SP, add_later, jnp.zeros_like(seg_total))
    gate_log = input_pre + suffix_of(log_forget) + later_sum[:, None, :]
    peak_log = by_axis(jnp.max(gate_log, axis=1), SP)
    scale = jnp.exp(gate_log - peak_log[:, None, :])
    pos_count = scale.shape[1]
    key_quartet = key_rows.reshape(seq_count, pos_count, head_count, key_size)
    value_four = values.reshape(seq_count, pos_count, head_count, -1)
    weighted_rows = (value_four * scale[..., None]).astype(jnp.bfloat16)
    memory_part = jnp.einsum(
        "slhk,slhv->shkv", key_quartet, weighted_rows, preferred_element_type=jnp.float32
    )
    normer_part = jnp.einsum("slh,slhk->shk", scale, key_quartet.astype(jnp.float32))
    memory_matrix, normer = (sum_at_owner(memory_part, SP, 3), sum_at_owner(normer_part, SP, 2))
    forget_new = jax.nn.log_sigmoid(new_forget_gate)
    new_peak = jnp.maximum(forget_new + peak_log, new_input_gate)
    old_scale = jnp.exp(forget_new + peak_log - new_peak)
    new_scale = jnp.exp(new_input_gate - new_peak)
    key_new = new_key.astype(jnp.float32)
    key_new_slice = lax.dynamic_slice_in_dim(key_new, sp_index * key_cols, key_cols, 2)
    value_new = new_value.astype(jnp.float32)
    memory_next = (
        old_scale[:, :, None, None] * memory_matrix
        + new_scale[:, :, None, None] * key_new[:, :, :, None] * value_new[:, :, None, :]
    )
    normer_next = old_scale[:, :, None] * normer + new_scale[:, :, None] * key_new_slice
    query = new_query.astype(jnp.float32)
    query_slice = lax.dynamic_slice_in_dim(query, sp_index * key_cols, key_cols, 2)
    numer = jnp.sum(query[:, :, :, None] * memory_next, axis=2)
    denom = over_axes(jnp.sum(query_slice * normer_next, axis=-1), SP)
    read = (numer / jnp.maximum(jnp.abs(denom), 1.0)[:, :, None]).astype(jnp.bfloat16)
    partial_value = jnp.einsum("shv,hvd->sd", read, out_weight, preferred_element_type=jnp.float32)
    read_out = sum_by_axis(partial_value, (("sp_0", "sp_1", "tp_0"), "tp_1"), 1).astype(
        jnp.bfloat16
    )
    return (memory_matrix.astype(jnp.bfloat16), normer.astype(jnp.bfloat16), peak_log, read_out)


def solution(mesh):
    torus = Mesh(mesh.devices.reshape(4, 4, 4, 2), ("sp_0", "sp_1", "tp_0", "tp_1"))
    in_specs = (
        P(None, SP, None),
        P(None, TP),
        P(None, TP),
        P(None, TP),
        P(None, TP),
        P(TP),
        P(None, TP),
        P(None, SP, TP),
        P(None, TP, None),
        P(None, TP, None),
        P(None, TP, SP),
        P(None, TP),
        P(None, TP),
        P(TP, SP, None),
    )
    out_specs = (P(None, TP, None, SP), P(None, TP, SP), P(None, TP), P(None, SP_TP))
    return jax.shard_map(body, mesh=torus, in_specs=in_specs, out_specs=out_specs, check_vma=False)
```

profile of v0, /device:TPU:1, one launch (start us, length us, event | category | flops | bytes accessed | tf_op | source)
XLA Modules:
  0.0 141.0 jit_solution(429639210175092399)
XLA Ops:
  0.7 10.7 %convolution_convert_fusion.1 = bf16[2048,128]{1,0:T(8,128)(2,1)S(1)} fusion(bf16[2048,4096]{1,0:T(8,128)(2,1)} %bitcast.56, bf16[4096,128]{1,0:T(8,128)(2,1)} %param.15), kind=kOutput, calls=%fused_computation.3 | convolution fusion | flops 2147745792 | bytes 18350080 | tf_op jit(solution)/shard_map/dot_general | solution.py:87
  11.4 1.3 collective-permute-start.1
  12.7 4.7 %collective-permute-start = (bf16[4,1,128]{2,1,0:T(2,128)(2,1)S(1)}, bf16[4,1,128]{2,1,0:T(2,128)(2,1)S(1)}, u32[]{:S(2)}, u32[]{:S(2)}) collective-permute-start(bf16[4,1,128]{2,1,0:T(2,128)(2,1)S(1)} %get-tuple-element.14), channel_id=1, source_target_pairs={{0,8},{8,16},{16,24},{24,32},{32,40},{40,48},{48,56},{56,64},{64,7... | collective-permute-start | bytes 3080 | tf_op jit(solution)/shard_map/ppermute | solution.py:22
  17.4 10.2 %fusion.1 = bf16[2048,4]{0,1:T(4,128)(2,1)S(1)} fusion(bf16[2048,4096]{1,0:T(8,128)(2,1)} %bitcast.57, bf16[4096,2]{0,1:T(2,128)(2,1)S(1)} %copy-done.2, bf16[4096,2]{0,1:T(2,128)(2,1)S(1)} %copy-done.3), kind=kOutput, calls=%fused_computation.5 | convolution fusion | flops 67182592 | bytes 16826368 | tf_op jit(solution)/shard_map/dot_general | solution.py:94
  28.0 0.6 broadcast_in_dim.15
  28.6 9.5 %all-to-all-start = ((f32[16,4,2]{1,2,0:T(2,128)}), f32[16,4,2]{1,2,0:T(2,128)S(1)}, u32[]{:S(2)}, u32[]{:S(2)}) async-start(f32[16,4,2]{1,2,0:T(2,128)} %broadcast_in_dim.15), calls=%async_computation | async-start | bytes 32768 | tf_op jit(solution)/shard_map/all_to_all | solution.py:30
  38.2 9.4 %fusion = f32[2048,256]{1,0:T(8,128)} fusion(bf16[2048,4096]{1,0:T(8,128)(2,1)} %bitcast.58, bf16[4096,256]{1,0:T(8,128)(2,1)S(1)} %copy-done), kind=kOutput, calls=%fused_computation.2 | convolution fusion | flops 4296015872 | bytes 20971520 | tf_op jit(solution)/shard_map/dot_general | solution.py:90
  47.6 3.4 %reshape.78 = f32[4,512,2,128]{3,2,1,0:T(2,128)} reshape(f32[2048,256]{1,0:T(8,128)} %fusion) | data formatting | bytes 4194304 | tf_op jit(solution)/shard_map/convert_element_type | solution.py:162
  51.0 2.4 %reduce-window.6 = f32[4,2,4,128]{3,2,1,0:T(4,128)S(1)} reduce-window(f32[4,2,4,128]{3,2,1,0:T(4,128)S(1)} %reshape.72, f32[]{:T(128)} %constant.15.clone.1), window={size=1x1x1x128 pad=0_0x0_0x0_0x127_0}, to_apply=%region_1.2 | reduce-window | flops 520192 | bytes 32772 | tf_op jit(solution)/shard_map/reduce-window
  53.6 0.7 reduce-window.9
  55.1 8.5 %pmax.14 = f32[4,2]{1,0:T(4,128)S(1)} all-reduce(f32[4,2]{1,0:T(4,128)S(1)} %fusion.21), channel_id=1, replica_groups=mesh['sp_0'=4,'sp_1'=4,'tp_0'=4,'tp_1'=2] {'sp_0'}, use_global_device_ids=true, to_apply=%region_4.5 | all-reduce | flops 8 | bytes 64 | tf_op jit(solution)/shard_map/pmax | solution.py:54
  63.6 8.6 %pmax.15 = f32[4,2]{1,0:T(4,128)S(1)} all-reduce(f32[4,2]{1,0:T(4,128)S(1)} %pmax.14), channel_id=1, replica_groups=mesh['sp_0'=4,'sp_1'=4,'tp_0'=4,'tp_1'=2] {'sp_1'}, use_global_device_ids=true, to_apply=%region_5.6 | all-reduce | flops 8 | bytes 64 | tf_op jit(solution)/shard_map/pmax | solution.py:54
  72.3 0.6 multiply_convert_fusion
  73.6 0.7 copy.63
  74.2 3.5 %all-to-all-start.2 = ((f32[16,4,2,4]{3,2,1,0:T(2,128)}), f32[16,4,2,4]{3,2,1,0:T(2,128)S(1)}, u32[]{:S(2)}, u32[]{:S(2)}) async-start(f32[16,4,2,4]{3,2,1,0:T(2,128)} %copy.63), calls=%async_computation.2 | async-start | bytes 131072 | tf_op jit(solution)/shard_map/all_to_all | solution.py:64
  77.7 2.8 %convolution_bitcast_fusion.1 = f32[16,4,2,64,8]{3,4,0,2,1:T(8,128)S(1)} fusion(bf16[4,512,2,64]{1,3,2,0:T(8,128)(2,1)S(1)} %bitcast.61, f32[4,512,2,128]{3,2,1,0:T(2,128)} %reshape.78, f32[4,512,2]{1,2,0:T(2,128)S(1)} %subtract_exponential_fusion), kind=kOutput, calls=%fused_computation.8 | convolution fusion | flops 68157440 | bytes 2899968 | tf_op jit(solution)/shard_map/slhk,slhv->shkv/dot_general | solution.py:163
  80.6 1.0 reshape.83
  81.6 2.5 %all-to-all-done.2 = f32[16,4,2,4]{3,2,1,0:T(2,128)S(1)} async-done(((f32[16,4,2,4]{3,2,1,0:T(2,128)}), f32[16,4,2,4]{3,2,1,0:T(2,128)S(1)}, u32[]{:S(2)}, u32[]{:S(2)}) %all-to-all-start.2) | async-done | bytes 2080 | tf_op jit(solution)/shard_map/all_to_all | solution.py:64
  84.2 4.1 %all-to-all-start.1 = ((f32[16,1,4096]{2,1,0:T(1,128)}), f32[16,1,4096]{2,1,0:T(1,128)S(1)}, u32[]{:S(2)}, u32[]{:S(2)}) async-start(f32[16,1,4096]{2,1,0:T(1,128)} %reshape.83), calls=%async_computation.1 | async-start | bytes 524288 | tf_op jit(solution)/shard_map/all_to_all | solution.py:64
  88.3 0.6 multiply_reduce_fusion.1
  88.9 8.5 %psum.14 = f32[4,2]{1,0:T(4,128)S(1)} all-reduce(f32[4,2]{1,0:T(4,128)S(1)} %get-tuple-element.22), channel_id=1, replica_groups=mesh['sp_0'=4,'sp_1'=4,'tp_0'=4,'tp_1'=2] {'sp_0'}, use_global_device_ids=true, to_apply=%region_10.11 | all-reduce | flops 8 | bytes 64 | tf_op jit(solution)/shard_map/psum | solution.py:70
  97.5 8.4 %psum.15 = f32[4,2]{1,0:T(4,128)S(1)} all-reduce(f32[4,2]{1,0:T(4,128)S(1)} %psum.14), channel_id=1, replica_groups=mesh['sp_0'=4,'sp_1'=4,'tp_0'=4,'tp_1'=2] {'sp_1'}, use_global_device_ids=true, to_apply=%region_11.12 | all-reduce | flops 8 | bytes 64 | tf_op jit(solution)/shard_map/psum | solution.py:70
  106.4 1.3 reduce.2
  107.9 0.7 multiply_reduce_fusion
  109.3 14.2 %all_to_all.25 = f32[2,1,8192]{2,1,0:T(1,128)S(1)} all-to-all(f32[2,1,8192]{2,1,0:T(1,128)S(1)} %reshape.85), channel_id=1, replica_groups=mesh['sp_0'=4,'sp_1'=4,'tp_0'=4,'tp_1'=2] {'tp_1'}, dimensions={0} | all-to-all | bytes 131072 | tf_op jit(solution)/shard_map/all_to_all | solution.py:64
  123.5 0.8 reduce.3
  124.6 0.7 reshape.87
  125.3 5.8 %all-to-all-start.4 = ((f32[64,1,128]{2,1,0:T(1,128)}), f32[64,1,128]{2,1,0:T(1,128)S(1)}, u32[]{:S(2)}, u32[]{:S(2)}) async-start(f32[64,1,128]{2,1,0:T(1,128)} %reshape.87), calls=%async_computation.4 | async-start | bytes 65536 | tf_op jit(solution)/shard_map/all_to_all | solution.py:77
  131.1 0.6 copy.72
  131.8 7.8 %all-to-all-done.4 = f32[64,1,128]{2,1,0:T(1,128)S(1)} async-done(((f32[64,1,128]{2,1,0:T(1,128)}), f32[64,1,128]{2,1,0:T(1,128)S(1)}, u32[]{:S(2)}, u32[]{:S(2)}) %all-to-all-start.4) | async-done | bytes 32800 | tf_op jit(solution)/shard_map/all_to_all | solution.py:77
  139.5 0.7 reduce.4
  140.4 0.6 reduce_sum.73
  (75 shorter events, 3.9 us)
Async XLA Ops:
  0.6 37.6 %copy-start = (bf16[4096,256]{1,0:T(8,128)(2,1)S(1)}, bf16[4096,256]{1,0:T(8,128)(2,1)}, u32[]{:S(2)}) copy-start(bf16[4096,256]{1,0:T(8,128)(2,1)} %param.16) | copy-start | bytes 6291460
  0.6 16.8 %copy-start.2 = (bf16[4096,2]{0,1:T(2,128)(2,1)S(1)}, bf16[4096,2]{0,1:T(2,128)(2,1)}, u32[]{:S(2)}) copy-start(bf16[4096,2]{0,1:T(2,128)(2,1)} %param.18) | copy-start | bytes 49156
  0.7 16.8 %copy-start.3 = (bf16[4096,2]{0,1:T(2,128)(2,1)S(1)}, bf16[4096,2]{0,1:T(2,128)(2,1)}, u32[]{:S(2)}) copy-start(bf16[4096,2]{0,1:T(2,128)(2,1)} %param.17) | copy-start | bytes 49156
  11.4 61.0 %collective-permute-start.1 = (bf16[4,1,128]{2,1,0:T(2,128)(2,1)S(1)}, bf16[4,1,128]{2,1,0:T(2,128)(2,1)S(1)}, u32[]{:S(2)}, u32[]{:S(2)}) collective-permute-start(bf16[4,1,128]{2,1,0:T(2,128)(2,1)S(1)} %get-tuple-element.15), channel_id=1, source_target_pairs={{8,0},{16,8},{24,16},{32,24},{40,32},{48,40},{56,48},{64,56},{72,6... | collective-permute-start | bytes 3080 | tf_op jit(solution)/shard_map/ppermute | solution.py:23
  12.7 15.0 %copy-start.4 = (f32[4,512,2]{1,2,0:T(2,128)S(1)}, f32[4,512,2]{1,2,0:T(2,128)}, u32[]{:S(2)}) copy-start(f32[4,512,2]{1,2,0:T(2,128)} %param.21) | copy-start | bytes 49156
  12.7 15.0 %copy-start.11 = (f32[2]{0:T(128)S(1)}, f32[2]{0:T(128)}, u32[]{:S(2)}) copy-start(f32[2]{0:T(128)} %param.19) | copy-start | bytes 28
  12.7 25.5 %copy-start.8 = (bf16[3,128]{1,0:T(4,128)(2,1)S(1)}, bf16[3,128]{1,0:T(4,128)(2,1)}, u32[]{:S(2)}) copy-start(bf16[3,128]{1,0:T(4,128)(2,1)} %param.20) | copy-start | bytes 2308
  12.7 59.6 %collective-permute-start = (bf16[4,1,128]{2,1,0:T(2,128)(2,1)S(1)}, bf16[4,1,128]{2,1,0:T(2,128)(2,1)S(1)}, u32[]{:S(2)}, u32[]{:S(2)}) collective-permute-start(bf16[4,1,128]{2,1,0:T(2,128)(2,1)S(1)} %get-tuple-element.14), channel_id=1, source_target_pairs={{0,8},{8,16},{16,24},{24,32},{32,40},{40,48},{48,56},{56,64},{64,7... | collective-permute-start | bytes 3080 | tf_op jit(solution)/shard_map/ppermute | solution.py:22
  28.6 26.1 %all-to-all-start = ((f32[16,4,2]{1,2,0:T(2,128)}), f32[16,4,2]{1,2,0:T(2,128)S(1)}, u32[]{:S(2)}, u32[]{:S(2)}) async-start(f32[16,4,2]{1,2,0:T(2,128)} %broadcast_in_dim.15), calls=%async_computation | async-start | bytes 32768 | tf_op jit(solution)/shard_map/all_to_all | solution.py:30
  47.6 6.8 %copy-start.6 = (bf16[4,2,8]{2,1,0:T(2,128)(2,1)S(1)}, bf16[4,2,8]{2,1,0:T(2,128)(2,1)}, u32[]{:S(2)}) copy-start(bf16[4,2,8]{2,1,0:T(2,128)(2,1)} %param.24) | copy-start | bytes 388
  47.6 6.8 %copy-start.9 = (f32[4,2]{0,1:T(2,128)S(1)}, f32[4,2]{0,1:T(2,128)}, u32[]{:S(2)}) copy-start(f32[4,2]{0,1:T(2,128)} %param.25) | copy-start | bytes 100
  47.6 6.9 %copy-start.10 = (f32[4,2]{0,1:T(2,128)S(1)}, f32[4,2]{0,1:T(2,128)}, u32[]{:S(2)}) copy-start(f32[4,2]{0,1:T(2,128)} %param.26) | copy-start | bytes 100
  47.6 7.0 %copy-start.7 = (bf16[4,2,64]{2,1,0:T(2,128)(2,1)S(1)}, bf16[4,2,64]{2,1,0:T(2,128)(2,1)}, u32[]{:S(2)}) copy-start(bf16[4,2,64]{2,1,0:T(2,128)(2,1)} %param.22) | copy-start | bytes 3076
  47.6 7.0 %copy-start.5 = (bf16[4,2,64]{2,1,0:T(2,128)(2,1)S(1)}, bf16[4,2,64]{2,1,0:T(2,128)(2,1)}, u32[]{:S(2)}) copy-start(bf16[4,2,64]{2,1,0:T(2,128)(2,1)} %param.23) | copy-start | bytes 3076
  74.2 10.0 %all-to-all-start.2 = ((f32[16,4,2,4]{3,2,1,0:T(2,128)}), f32[16,4,2,4]{3,2,1,0:T(2,128)S(1)}, u32[]{:S(2)}, u32[]{:S(2)}) async-start(f32[16,4,2,4]{3,2,1,0:T(2,128)} %copy.63), calls=%async_computation.2 | async-start | bytes 131072 | tf_op jit(solution)/shard_map/all_to_all | solution.py:64
  80.5 28.1 %copy-start.1 = (bf16[2,8,4096]{2,1,0:T(8,128)(2,1)S(1)}, bf16[2,8,4096]{2,1,0:T(8,128)(2,1)}, u32[]{:S(2)}) copy-start(bf16[2,8,4096]{2,1,0:T(8,128)(2,1)} %param.27) | copy-start | bytes 393220
  84.2 21.7 %all-to-all-start.1 = ((f32[16,1,4096]{2,1,0:T(1,128)}), f32[16,1,4096]{2,1,0:T(1,128)S(1)}, u32[]{:S(2)}, u32[]{:S(2)}) async-start(f32[16,1,4096]{2,1,0:T(1,128)} %reshape.83), calls=%async_computation.1 | async-start | bytes 524288 | tf_op jit(solution)/shard_map/all_to_all | solution.py:64
  125.3 14.2 %all-to-all-start.4 = ((f32[64,1,128]{2,1,0:T(1,128)}), f32[64,1,128]{2,1,0:T(1,128)S(1)}, u32[]{:S(2)}, u32[]{:S(2)}) async-start(f32[64,1,128]{2,1,0:T(1,128)} %reshape.87), calls=%async_computation.4 | async-start | bytes 65536 | tf_op jit(solution)/shard_map/all_to_all | solution.py:77
where the time goes:
time: 142 us; the launch traced here: 141 us
  blocking collectives  48.2 us (34%)
  matrix products  33.6 us (24%)
  starting transfers between devices  28.9 us (20%)
  waiting for transfers between devices  10.3 us (7%)
  local copies, waits for them, and re-layouts  9.54 us (7%)
  other arithmetic  9.47 us (7%)
    pmax x2, blocking collectives, by_axis(): return functools.reduce(lax.pmax, axes, shard)  17.1 us
    psum x2, blocking collectives, over_axes(): shard = lax.psum(shard, axis)  16.9 us
    all_to_all x1, blocking collectives, sum_at_owner(): lax.all_to_all(in_blocks(shard, dim, devices), axis, 0, 0, tiled=True)  14.2 us
    dot_general x1, matrix products, project(): jnp.dot(flat_rows, key_weight, preferred_element_type=jnp.float32)  10.7 us
    dot_general x1, matrix products, project(): jnp.dot(flat_rows, gate_weight, preferred_element_type=jnp.float32)  10.2 us
    all_to_all x1, starting transfers between devices, copy_for_each(): return lax.all_to_all(copies, axis, split_axis=0, concat_axis=0, tiled=True)  9.52 us
    dot_general x1, matrix products, project(): jnp.dot(flat_rows, value_weight, preferred_element_type=jnp.float32)  9.43 us
    all_to_all x1, waiting for transfers between devices, sum_by_axis(): return jnp.sum(lax.all_to_all(own, far, 0, 0, tiled=True), axis=0)  7.78 us
  transfers between devices with their start and end apart: 6, of which 2 were waited for; matrix products, arithmetic and copies ran while one was open for 24% of the time, Pallas kernels for 0%

commit v1 on v0

v1 whole, which is shorter than its diff:
```python
import jax
import jax.numpy as jnp
from jax import lax
from jax.experimental import pallas as pl
from jax.experimental.pallas import tpu as pltpu
from jax.sharding import Mesh
from jax.sharding import PartitionSpec as P

KEY_DIM = 64
SP = ("sp_0", "sp_1")
SP_TP = ("sp_0", "sp_1", "tp_0", "tp_1")
TP = ("tp_0", "tp_1")
LANES = 128
SEQ_ROWS = 16
F32 = jnp.float32
BF16 = jnp.bfloat16


def lane_iota(shape):
    return lax.broadcasted_iota(jnp.int32, shape, len(shape) - 1)


def row_iota(shape):
    return lax.broadcasted_iota(jnp.int32, shape, 0)


def log_sigmoid(x):
    return jnp.minimum(x, 0.0) - jnp.log1p(jnp.exp(-jnp.abs(x)))


def key_activation(mixed):
    return (mixed * jax.nn.sigmoid(mixed) * KEY_DIM ** (-0.5)).astype(BF16)


def suffix_after(x):
    length = x.shape[-1]
    lanes = lane_iota(x.shape)

    def ahead(y, by):
        return jnp.where(lanes < length - by, pltpu.roll(y, length - by, y.ndim - 1), 0.0)

    total = ahead(x, 1)
    by = 1
    while by < length:
        total = total + ahead(total, by)
        by *= 2
    return total


def state_kernel(bias_ref, x_ref, wk_ref, wv_ref, wi_ref, wf_ref, taps_ref, extra_ref, out_ref, w_ref, spread_ref):
    s = pl.program_id(0)
    rows = x_ref.shape[1]
    width = x_ref.shape[2]
    half = lane_iota((1, LANES)) < KEY_DIM

    @pl.when(s == 0)
    def _():
        w_ref[:, :LANES] = wk_ref[...]
        pad = jnp.zeros((6, LANES), F32)
        tail = jnp.zeros((LANES - 16, LANES), F32)
        for c in range(width // LANES):
            cols = slice(c * LANES, (c + 1) * LANES)
            gates = jnp.concatenate(
                [wi_ref[:, cols].astype(F32), pad, wf_ref[:, cols].astype(F32), pad, tail], axis=0
            )
            w_ref[cols, LANES:] = gates.T.astype(BF16)
        spot = lax.broadcasted_iota(jnp.int32, spread_ref.shape, 0)
        lane = lane_iota(spread_ref.shape)
        goal = (spot // LANES) * 8 + spot % 8
        spread_ref[...] = jnp.where(goal == lane, 1.0, 0.0).astype(BF16)

    x = x_ref[0]
    key_gate = jnp.dot(x, w_ref[...], preferred_element_type=F32)
    values = jnp.dot(x, wv_ref[...], preferred_element_type=F32).astype(BF16)
    raw_bf = key_gate[:, :LANES].astype(BF16)
    raw = raw_bf.astype(F32)
    gates = key_gate[:, LANES:].T
    input_pre = gates[0:2].astype(BF16).astype(F32)
    forget_pre = gates[8:10].astype(BF16).astype(F32)
    bias = jnp.where(row_iota((2, 1)) == 0, bias_ref[0], bias_ref[1])
    log_forget = log_sigmoid(forget_pre + bias) + extra_ref[0]
    gate_log = input_pre + suffix_after(log_forget)
    peak = jnp.max(gate_log, axis=1, keepdims=True)
    seg_total = jnp.sum(log_forget, axis=1, keepdims=True)
    scale = jnp.exp(gate_log - peak)

    taps = taps_ref[...].astype(F32)
    before = pltpu.roll(raw, 1, 0)
    after = pltpu.roll(raw, rows - 1, 0)
    mixed = taps[0:1] * before + taps[1:2] * raw + taps[2:3] * after
    place = row_iota((rows, 1))
    inner = (place > 0) & (place < rows - 1)
    key_rows = jnp.where(inner, key_activation(mixed).astype(F32), 0.0)
    key_t = key_rows.T
    scaled_t = jnp.concatenate([key_t[:KEY_DIM] * scale[0:1], key_t[KEY_DIM:] * scale[1:2]], axis=0)
    memory = jnp.dot(scaled_t.astype(BF16), values, preferred_element_type=F32)
    memory = jnp.concatenate([memory[:KEY_DIM, :LANES], memory[KEY_DIM:, LANES:]], axis=0).T
    owners = LANES // 8
    base = pl.multiple_of(s * SEQ_ROWS, 8)
    out_ref[:, pl.ds(base, 8), :] = memory.reshape(owners, 8, LANES)

    high = scale.astype(BF16).astype(F32)
    middle = (scale - high).astype(BF16).astype(F32)
    low = scale - high - middle
    pieces = jnp.concatenate([high, middle, low, jnp.zeros_like(low)], axis=0).astype(BF16)
    norm = jnp.dot(pieces, key_rows.astype(BF16), preferred_element_type=F32)
    norm = jnp.where(half, norm[0:1] + norm[2:3] + norm[4:5], norm[1:2] + norm[3:4] + norm[5:6])

    ends = []
    for at in (0, rows - 1):
        for h in range(2):
            row = values[at : at + 1, h * LANES : (h + 1) * LANES].astype(F32)
            ends.append(row * scale[h : h + 1, at : at + 1])
    ends = jnp.concatenate(ends, axis=1)
    spot = lax.broadcasted_iota(jnp.int32, (owners, ends.shape[1]), 1)
    mine = (spot % LANES) // 8 == row_iota((owners, 1))
    picked = jnp.where(mine, ends, 0.0).astype(BF16)
    by_owner = jnp.dot(picked, spread_ref[...], preferred_element_type=F32)
    lane = lane_iota((1, LANES))
    last = jnp.zeros((1, LANES), F32)
    for p, at in enumerate((0, rows - 1)):
        for h in range(2):
            last = jnp.where(lane == 32 + 2 * p + h, scale[h : h + 1, at : at + 1], last)
    shared = jnp.concatenate(
        [
            raw[0:2],
            raw[rows - 2 : rows],
            norm,
            jnp.where(half, peak[0:1], peak[1:2]),
            jnp.where(half, seg_total[0:1], seg_total[1:2]),
            last,
        ],
        axis=0,
    )
    by_owner = jnp.where(row_iota((8, LANES))[None] == 7, by_owner[:, None, :], 0.0)
    out_ref[:, pl.ds(base + 8, 8), :] = shared[None] + by_owner


def prompt_states(prompt, key_weight, value_weight, input_gate_t, forget_gate_t, forget_bias, key_taps, extra_t):
    seqs, rows, width = prompt.shape
    owners = LANES // 8
    whole = lambda a: pl.BlockSpec(a.shape, lambda s: (0,) * a.ndim)
    return pl.pallas_call(
        state_kernel,
        grid=(seqs,),
        in_specs=[
            pl.BlockSpec(memory_space=pltpu.SMEM),
            pl.BlockSpec((1, rows, width), lambda s: (s, 0, 0)),
            whole(key_weight),
            whole(value_weight),
            whole(input_gate_t),
            whole(forget_gate_t),
            whole(key_taps),
            pl.BlockSpec((1, 2, rows), lambda s: (s, 0, 0)),
        ],
        out_specs=pl.BlockSpec((owners, seqs * SEQ_ROWS, LANES), lambda s: (0, 0, 0)),
        out_shape=jax.ShapeDtypeStruct((owners, seqs * SEQ_ROWS, LANES), F32),
        scratch_shapes=[pltpu.VMEM((width, 2 * LANES), BF16), pltpu.VMEM((4 * LANES, LANES), BF16)],
        compiler_params=pltpu.CompilerParams(vmem_limit_bytes=48 * 1024 * 1024),
        name="prompt_states",
    )(forget_bias, prompt, key_weight, value_weight, input_gate_t, forget_gate_t, key_taps, extra_t)


def read_kernel(
    index_ref, forget_ref, gate_ref, parts_ref, taps_ref, query_ref, key_ref, value_ref, weight_ref,
    memory_out, norm_out, peak_out, sent_out,
):
    devices = parts_ref.shape[0]
    seqs = query_ref.shape[0]
    half = lane_iota((1, LANES)) < KEY_DIM
    device = row_iota((devices, 1))
    taps = taps_ref[...].astype(F32)
    down = lambda y, by: jnp.where(device < devices - by, pltpu.roll(y, devices - by, 0), 0.0)
    reads = [jnp.zeros((8, LANES), F32), jnp.zeros((8, LANES), F32)]
    peaks = jnp.zeros((2, seqs), F32)
    for s in range(seqs):
        base = s * SEQ_ROWS
        row = lambda r: parts_ref[:, base + 8 + r, :]
        later = down(row(6), 1)
        for by in (1, 2, 4, 8):
            later = later + down(later, by)
        level = row(5) + later
        peak = jnp.max(level, axis=0, keepdims=True)
        factor = jnp.exp(level - peak)
        before = jnp.where(device > 0, pltpu.roll(row(3), 1, 0), 0.0)
        first = key_activation(taps[0:1] * before + taps[1:2] * row(0) + taps[2:3] * row(1)).astype(F32)
        last = key_activation(taps[0:1] * row(2) + taps[1:2] * row(3) + taps[2:3] * down(row(0), 1)).astype(F32)
        ends = row(7)
        contract = (((0,), (0,)), ((), ()))
        at_first, at_last = (
            lax.dot_general(ends, rows * factor, contract, precision=lax.Precision.HIGHEST, preferred_element_type=F32)
            for rows in (first, last)
        )
        edge = jnp.where(half, at_first[0:8] + at_last[16:24], at_first[8:16] + at_last[24:32])
        norm_edge = jnp.where(half, at_first[32:33] + at_last[34:35], at_first[33:34] + at_last[35:36])
        memory = edge + jnp.sum(parts_ref[:, base : base + 8, :] * factor[:, None, :], axis=0)
        norm = norm_edge + jnp.sum(row(4) * factor, axis=0, keepdims=True)
        memory_bf = memory.astype(BF16)
        memory_out[s, 0] = memory_bf[:, :KEY_DIM]
        memory_out[s, 1] = memory_bf[:, KEY_DIM:]
        own = pltpu.roll(norm, LANES - index_ref[0] * 4, 1)
        norm_out[s, 0:1, :] = own[:, 0:4].astype(BF16)
        norm_out[s, 1:2, :] = own[:, KEY_DIM : KEY_DIM + 4].astype(BF16)

        forget = log_sigmoid(jnp.where(half, forget_ref[s, 0], forget_ref[s, 1]))
        gate = jnp.where(half, gate_ref[s, 0], gate_ref[s, 1])
        new_peak = jnp.maximum(forget + peak, gate)
        old_scale = jnp.exp(forget + peak - new_peak)
        new_scale = jnp.exp(gate - new_peak)
        query = query_ref[s : s + 1]
        new_key = new_scale * key_ref[s : s + 1]
        numer = query * (old_scale * memory + new_key * value_ref[s])
        denom = query * (old_scale * norm + new_key)
        spot = lane_iota((8, LANES))
        for h in range(2):
            side = half if h == 0 else jnp.logical_not(half)
            top = jnp.sum(jnp.where(side, numer, 0.0), axis=1, keepdims=True)
            bottom = jnp.sum(jnp.where(side, denom, 0.0), axis=1, keepdims=True)
            read = top / jnp.maximum(jnp.abs(bottom), 1.0)
            reads[h] = jnp.where((spot & 3) == s, read, reads[h])
            mark = (lane_iota(peaks.shape) == s) & (row_iota(peaks.shape) == h)
            peaks = jnp.where(mark, peak[:, h * KEY_DIM : h * KEY_DIM + 1], peaks)
    peak_out[...] = peaks
    read_rows = jnp.concatenate(reads, axis=0).T[0:8].astype(BF16)
    partial = jnp.dot(read_rows, weight_ref[...], preferred_element_type=F32)
    sub = row_iota((8, LANES))
    block = lane_iota((8, LANES)) // 32
    for m in range(partial.shape[1] // (2 * LANES)):
        low = partial[:, 2 * m * LANES : (2 * m + 1) * LANES]
        high = partial[:, (2 * m + 1) * LANES : (2 * m + 2) * LANES]
        both = jnp.where(sub < 4, low, high)
        out = jnp.zeros_like(both)
        for r in range(4):
            moved = pltpu.roll(both, 32 * r, 1) if r else both
            if r:
                near = pltpu.roll(moved, 8 - r, 0)
                wrap = pltpu.roll(moved, 4 - r, 0)
                moved = jnp.where((sub & 3) + r < 4, near, wrap)
            out = jnp.where(block == (((sub & 3) + r) & 3), moved, out)
        sent_out[8 * m : 8 * m + 8, :] = out


def first_read(index, forget, gate, parts, taps, query, key, value, weight):
    seqs = query.shape[0]
    vmem = pl.BlockSpec(memory_space=pltpu.VMEM)
    smem = pl.BlockSpec(memory_space=pltpu.SMEM)
    devices_all = weight.shape[1] // 32
    return pl.pallas_call(
        read_kernel,
        in_specs=[smem, smem, smem] + [vmem] * 6,
        out_specs=[vmem] * 4,
        out_shape=[
            jax.ShapeDtypeStruct((seqs, 2, 8, KEY_DIM), BF16),
            jax.ShapeDtypeStruct((seqs, 2, 4), BF16),
            jax.ShapeDtypeStruct((2, seqs), F32),
            jax.ShapeDtypeStruct((devices_all, LANES), F32),
        ],
        compiler_params=pltpu.CompilerParams(vmem_limit_bytes=32 * 1024 * 1024),
        name="first_read",
    )(index, forget, gate, parts, taps, query, key, value, weight)


def sum_kernel(parts_ref, out_ref):
    total = jnp.sum(parts_ref[...], axis=0, keepdims=True)
    for s in range(out_ref.shape[0]):
        out_ref[s : s + 1, :] = total[:, 32 * s : 32 * s + 32].astype(BF16)


def sum_parts(parts, seqs):
    vmem = pl.BlockSpec(memory_space=pltpu.VMEM)
    return pl.pallas_call(
        sum_kernel,
        in_specs=[vmem],
        out_specs=vmem,
        out_shape=jax.ShapeDtypeStruct((seqs, 32), BF16),
        name="sum_parts",
    )(parts)


def body(
    prompt, key_weight, value_weight, input_gate_weight, forget_gate_weight, forget_bias, key_taps,
    extra_decay, new_query, new_key, new_value, new_input_gate, new_forget_gate, out_weight,
):
    seqs = prompt.shape[0]
    index = lax.axis_index(SP).reshape(1)
    parts = prompt_states(
        prompt, key_weight, value_weight, input_gate_weight.T, forget_gate_weight.T, forget_bias,
        key_taps, extra_decay.transpose(0, 2, 1),
    )
    query = new_query.astype(F32).reshape(seqs, LANES)
    key = new_key.astype(F32).reshape(seqs, LANES)
    value = jnp.repeat(new_value.astype(F32).transpose(0, 2, 1), KEY_DIM, axis=2)
    parts = lax.all_to_all(parts, SP, 0, 0, tiled=True)
    memory, norm, peak, sent = first_read(
        index, new_forget_gate, new_input_gate, parts, key_taps, query, key, value,
        out_weight.reshape(-1, out_weight.shape[2]),
    )
    got = lax.all_to_all(sent.reshape(-1, 1, LANES), SP_TP, 0, 0, tiled=True)
    read_out = sum_parts(got.reshape(-1, LANES), seqs)
    return memory.swapaxes(2, 3), norm, peak.T, read_out


def solution(mesh):
    torus = Mesh(mesh.devices.reshape(4, 4, 4, 2), ("sp_0", "sp_1", "tp_0", "tp_1"))
    in_specs = (
        P(None, SP, None), P(None, TP), P(None, TP), P(None, TP), P(None, TP), P(TP), P(None, TP),
        P(None, SP, TP), P(None, TP, None), P(None, TP, None), P(None, TP, SP), P(None, TP), P(None, TP),
        P(TP, SP, None),
    )
    out_specs = (P(None, TP, None, SP), P(None, TP, SP), P(None, TP), P(None, SP_TP))
    return jax.shard_map(body, mesh=torus, in_specs=in_specs, out_specs=out_specs, check_vma=False)
```

time: 142 us -> 64 us (0.45)
  matrix products: 33.6 us -> 0 us
  blocking collectives: 48.2 us -> 17.1 us
  Pallas kernels: 0 us -> 20.5 us
  starting transfers between devices: 28.9 us -> 8.42 us
  other arithmetic: 9.47 us -> 0.01 us
  local copies, waits for them, and re-layouts: 9.54 us -> 6.97 us
    dot_general x6 -> x0, matrix products: 33.6 us -> none  [the longest x1 10.7 us: project(): jnp.dot(flat_rows, key_weight, preferred_element_type=jnp.float32)]
    pallas_call x0 -> x3, Pallas kernels: none -> 20.5 us  [the longest x1 17 us: prompt_states(): pl.pallas_call(state_kernel, grid=(seqs,), in_specs=[pl.BlockSpec(memory_...]
    pmax x2 -> x0, blocking collectives: 17.1 us -> none  [by_axis(): return functools.reduce(lax.pmax, axes, shard)]
    psum x2 -> x0, blocking collectives: 16.9 us -> none  [over_axes(): shard = lax.psum(shard, axis)]
    all_to_all x4 -> x1, starting transfers between devices: 22.9 us -> 8.42 us  [body(): parts = lax.all_to_all(parts, SP, 0, 0, tiled=True)]
    ppermute x2 -> x0, starting transfers between devices: 5.99 us -> none  [the longest x1 4.7 us: with_halo(): before = lax.ppermute(last, axis, up)]
    convert_element_type x2 -> x0, local copies, waits for them, and re-layouts: 3.57 us -> none  [the longest x1 3.36 us: body(): weighted_rows = (value_four * scale[..., None]).astype(jnp.bfloat16)]
    unnamed x33 -> x30, local copies, waits for them, and re-layouts: 3.25 us -> 6.52 us
  transfers between devices with their start and end apart: 6 -> 1, of which waited for: 2 -> 1; matrix products, arithmetic and copies ran while one was open for 24% -> 1% of each run, Pallas kernels for 0% -> 0%
where the time goes in v1:
time: 64 us; the launch traced here: 63.5 us
  Pallas kernels  20.5 us (32%)
  blocking collectives  17.1 us (27%)
  waiting for transfers between devices  9.75 us (15%)
  starting transfers between devices  8.42 us (13%)
  local copies, waits for them, and re-layouts  6.97 us (11%)
  between operations  0.73 us (1%)
    all_to_all x1, blocking collectives, body(): got = lax.all_to_all(sent.reshape(-1, 1, LANES), SP_TP, 0, 0, tiled=True)  17.1 us
    pallas_call x1, Pallas kernels, prompt_states(): pl.pallas_call(state_kernel, grid=(seqs,), in_specs=[pl.BlockSpec(memory_...  17 us
    all_to_all x1, waiting for transfers between devices, body(): parts = lax.all_to_all(parts, SP, 0, 0, tiled=True)  9.75 us
    all_to_all x1, starting transfers between devices, body(): parts = lax.all_to_all(parts, SP, 0, 0, tiled=True)  8.42 us
    unnamed x30, local copies, waits for them, and re-layouts  6.52 us
    pallas_call x1, Pallas kernels, first_read(): pl.pallas_call(read_kernel, in_specs=[smem, smem, smem] + [vmem] * 6, out...  2.02 us
    pallas_call x1, Pallas kernels, sum_parts(): pl.pallas_call(sum_kernel, in_specs=[vmem], out_specs=vmem, out_shape=jax...  1.5 us
  transfers between devices with their start and end apart: 1, of which 1 were waited for; matrix products, arithmetic and copies ran while one was open for 1% of the time, Pallas kernels for 0%

profile of v1, /device:TPU:1, one launch (start us, length us, event | category | flops | bytes accessed | tf_op | source)
XLA Modules:
  0.0 63.5 jit_solution(9168664289148840182)
XLA Ops:
  0.6 0.0 copy-start.7
  0.6 0.0 copy-start.9
  0.7 0.0 copy-start.10
  0.7 0.0 copy-start
  0.7 1.6 %copy-done = bf16[4096,256]{1,0:T(8,128)(2,1)S(1)} copy-done((bf16[4096,256]{1,0:T(8,128)(2,1)S(1)}, bf16[4096,256]{1,0:T(8,128)(2,1)}, u32[]{:S(2)}) %copy-start) | copy-done | bytes 2097176
  2.3 0.0 copy-start.1
  2.3 1.2 %copy-done.1 = bf16[4096,128]{1,0:T(8,128)(2,1)S(1)} copy-done((bf16[4096,128]{1,0:T(8,128)(2,1)S(1)}, bf16[4096,128]{1,0:T(8,128)(2,1)}, u32[]{:S(2)}) %copy-start.1) | copy-done | bytes 1048600
  3.5 0.7 %copy-done.3 = bf16[4096,2]{0,1:T(2,128)(2,1)S(1)} copy-done((bf16[4096,2]{0,1:T(2,128)(2,1)S(1)}, bf16[4096,2]{0,1:T(2,128)(2,1)}, u32[]{:S(2)}) %copy-start.3) | copy-done | bytes 16408
  4.2 0.7 %copy-done.4 = bf16[4096,2]{0,1:T(2,128)(2,1)S(1)} copy-done((bf16[4096,2]{0,1:T(2,128)(2,1)S(1)}, bf16[4096,2]{0,1:T(2,128)(2,1)}, u32[]{:S(2)}) %copy-start.4) | copy-done | bytes 16408
  4.9 0.7 %copy-done.5 = f32[4,512,2]{1,2,0:T(2,128)S(1)} copy-done((f32[4,512,2]{1,2,0:T(2,128)S(1)}, f32[4,512,2]{1,2,0:T(2,128)}, u32[]{:S(2)}) %copy-start.5) | copy-done | bytes 16408
  5.7 0.7 %copy-done.6 = bf16[3,128]{1,0:T(4,128)(2,1)S(1)} copy-done((bf16[3,128]{1,0:T(4,128)(2,1)S(1)}, bf16[3,128]{1,0:T(4,128)(2,1)}, u32[]{:S(2)}) %copy-start.6) | copy-done | bytes 792
  6.3 0.7 %copy-done.8 = f32[2]{0:T(128)S(1)} copy-done((f32[2]{0:T(128)S(1)}, f32[2]{0:T(128)}, u32[]{:S(2)}) %copy-start.8) | copy-done | bytes 32
  7.0 17.0 %prompt_states.1 = f32[16,64,128]{2,1,0:T(8,128)} custom-call(f32[2]{0:T(128)S(1)} %copy-done.8, bf16[4,512,4096]{2,1,0:T(8,128)(2,1)} %x_ref.1, bf16[4096,128]{1,0:T(8,128)(2,1)S(1)} %copy-done.1, bf16[4096,256]{1,0:T(8,128)(2,1)S(1)} %copy-done, bf16[2,4096]{1,0:T(2,128)(2,1)S(1)} %bitcast.15, bf16[2,4096]{1,0:T(2,128)(2,1)S(1)} %bitcast.16, ...), custom_call_target="tpu_custom_call" | custom-call | tf_op jit(solution)/shard_map/prompt_states/pallas_call | solution.py:143
  24.0 8.4 %all-to-all-start = ((f32[16,64,128]{2,1,0:T(8,128)}), f32[16,64,128]{2,1,0:T(8,128)S(1)}, u32[]{:S(2)}, u32[]{:S(2)}) async-start(f32[16,64,128]{2,1,0:T(8,128)} %prompt_states.1), calls=%async_computation | async-start | bytes 1048576 | tf_op jit(solution)/shard_map/all_to_all | solution.py:293
  32.4 0.0 copy-done.9
  32.4 0.1 copy.21
  32.5 0.1 broadcast_in_dim.3
  32.6 0.1 reshape.38.value_ref
  32.7 0.0 copy-done.12
  32.7 0.1 copy.22.forget_ref
  32.8 0.0 copy-done.13
  32.8 0.1 copy.23.gate_ref
  32.9 0.0 copy-done.10
  32.9 0.1 reshape.43.query_ref
  33.0 0.0 copy-done.11
  33.0 0.1 reshape.45.key_ref
  33.1 9.8 %all-to-all-done.parts_ref = f32[16,64,128]{2,1,0:T(8,128)S(1)} async-done(((f32[16,64,128]{2,1,0:T(8,128)}), f32[16,64,128]{2,1,0:T(8,128)S(1)}, u32[]{:S(2)}, u32[]{:S(2)}) %all-to-all-start) | async-done | bytes 524320 | tf_op jit(solution)/shard_map/all_to_all | solution.py:293
  42.8 0.0 copy-done.7
  42.8 0.0 copy-done.2
  42.8 2.0 %first_read.1 = (bf16[4,2,8,64]{3,2,1,0:T(8,128)(2,1)}, bf16[4,2,4]{2,1,0:T(2,128)(2,1)}, f32[2,4]{1,0:T(2,128)}, f32[128,128]{1,0:T(8,128)S(1)}) custom-call(s32[1]{0:T(128)} %bitcast.index_ref, f32[4,2]{1,0:T(4,128)S(1)} %copy.22.forget_ref, f32[4,2]{1,0:T(4,128)S(1)} %copy.23.gate_ref, f32[16,64,128]{2,1,0:T(8,128)S(1)} %all-to-all-done.parts_ref, ...), custom_call_target="tpu_custom_call" | custom-call | tf_op jit(solution)/shard_map/first_read/pallas_call | solution.py:248
  44.9 17.1 %all_to_all.10 = f32[128,1,128]{2,1,0:T(1,128)} all-to-all(f32[128,1,128]{2,1,0:T(1,128)S(1)} %bitcast.14), channel_id=1, replica_groups=mesh['sp_0'=4,'sp_1'=4,'tp_0'=4,'tp_1'=2] {'sp_0','sp_1','tp_0','tp_1'}, dimensions={0} | all-to-all | bytes 131072 | tf_op jit(solution)/shard_map/all_to_all | solution.py:298
  62.0 1.5 %sum_parts.1 = bf16[4,32]{1,0:T(4,128)(2,1)} custom-call(f32[128,128]{1,0:T(8,128)} %bitcast.18), custom_call_target="tpu_custom_call" | custom-call | tf_op jit(solution)/shard_map/sum_parts/pallas_call | solution.py:271
  (10 shorter events, 0.0 us)
Async XLA Ops:
  0.6 42.2 %copy-start.7 = (bf16[3,128]{1,0:T(4,128)(2,1)S(1)}, bf16[3,128]{1,0:T(4,128)(2,1)}, u32[]{:S(2)}) copy-start(bf16[3,128]{1,0:T(4,128)(2,1)} %taps_ref.3) | copy-start | bytes 2308
  0.6 31.8 %copy-start.9 = (bf16[4,2,8]{2,1,0:T(2,128)(2,1)S(1)}, bf16[4,2,8]{2,1,0:T(2,128)(2,1)}, u32[]{:S(2)}) copy-start(bf16[4,2,8]{2,1,0:T(2,128)(2,1)} %param.24) | copy-start | bytes 388
  0.7 32.3 %copy-start.10 = (bf16[4,2,64]{2,1,0:T(2,128)(2,1)S(1)}, bf16[4,2,64]{2,1,0:T(2,128)(2,1)}, u32[]{:S(2)}) copy-start(bf16[4,2,64]{2,1,0:T(2,128)(2,1)} %param.22) | copy-start | bytes 3076
  0.7 1.6 %copy-start = (bf16[4096,256]{1,0:T(8,128)(2,1)S(1)}, bf16[4096,256]{1,0:T(8,128)(2,1)}, u32[]{:S(2)}) copy-start(bf16[4096,256]{1,0:T(8,128)(2,1)} %wv_ref.1) | copy-start | bytes 6291460
  2.3 1.2 %copy-start.1 = (bf16[4096,128]{1,0:T(8,128)(2,1)S(1)}, bf16[4096,128]{1,0:T(8,128)(2,1)}, u32[]{:S(2)}) copy-start(bf16[4096,128]{1,0:T(8,128)(2,1)} %wk_ref.1) | copy-start | bytes 3145732
  3.5 0.7 %copy-start.3 = (bf16[4096,2]{0,1:T(2,128)(2,1)S(1)}, bf16[4096,2]{0,1:T(2,128)(2,1)}, u32[]{:S(2)}) copy-start(bf16[4096,2]{0,1:T(2,128)(2,1)} %param.17) | copy-start | bytes 49156
  4.2 0.7 %copy-start.4 = (bf16[4096,2]{0,1:T(2,128)(2,1)S(1)}, bf16[4096,2]{0,1:T(2,128)(2,1)}, u32[]{:S(2)}) copy-start(bf16[4096,2]{0,1:T(2,128)(2,1)} %param.18) | copy-start | bytes 49156
  4.9 0.7 %copy-start.5 = (f32[4,512,2]{1,2,0:T(2,128)S(1)}, f32[4,512,2]{1,2,0:T(2,128)}, u32[]{:S(2)}) copy-start(f32[4,512,2]{1,2,0:T(2,128)} %param.21) | copy-start | bytes 49156
  5.7 0.7 %copy-start.6 = (bf16[3,128]{1,0:T(4,128)(2,1)S(1)}, bf16[3,128]{1,0:T(4,128)(2,1)}, u32[]{:S(2)}) copy-start(bf16[3,128]{1,0:T(4,128)(2,1)} %taps_ref.3) | copy-start | bytes 2308
  6.3 0.7 %copy-start.8 = (f32[2]{0:T(128)S(1)}, f32[2]{0:T(128)}, u32[]{:S(2)}) copy-start(f32[2]{0:T(128)} %bias_ref.1) | copy-start | bytes 28
  7.0 25.7 %copy-start.12 = (f32[4,2]{0,1:T(2,128)S(1)}, f32[4,2]{0,1:T(2,128)}, u32[]{:S(2)}) copy-start(f32[4,2]{0,1:T(2,128)} %param.26) | copy-start | bytes 100
  7.0 25.8 %copy-start.13 = (f32[4,2]{0,1:T(2,128)S(1)}, f32[4,2]{0,1:T(2,128)}, u32[]{:S(2)}) copy-start(f32[4,2]{0,1:T(2,128)} %param.25) | copy-start | bytes 100
  7.0 26.0 %copy-start.11 = (bf16[4,2,64]{2,1,0:T(2,128)(2,1)S(1)}, bf16[4,2,64]{2,1,0:T(2,128)(2,1)}, u32[]{:S(2)}) copy-start(bf16[4,2,64]{2,1,0:T(2,128)(2,1)} %param.23) | copy-start | bytes 3076
  7.0 35.8 %copy-start.2 = (bf16[2,8,4096]{2,1,0:T(8,128)(2,1)S(1)}, bf16[2,8,4096]{2,1,0:T(8,128)(2,1)}, u32[]{:S(2)}) copy-start(bf16[2,8,4096]{2,1,0:T(8,128)(2,1)} %param.27) | copy-start | bytes 393220
  24.0 18.9 %all-to-all-start = ((f32[16,64,128]{2,1,0:T(8,128)}), f32[16,64,128]{2,1,0:T(8,128)S(1)}, u32[]{:S(2)}, u32[]{:S(2)}) async-start(f32[16,64,128]{2,1,0:T(8,128)} %prompt_states.1), calls=%async_computation | async-start | bytes 1048576 | tf_op jit(solution)/shard_map/all_to_all | solution.py:293

commit v2 on v1

v2 whole, which is shorter than its diff:
```python
import jax
import jax.numpy as jnp
from jax import lax
from jax.experimental import pallas as pl
from jax.experimental.pallas import tpu as pltpu
from jax.sharding import Mesh
from jax.sharding import PartitionSpec as P

KEY_DIM = 64
SP = ("sp_0", "sp_1")
SP_TP = ("sp_0", "sp_1", "tp_0", "tp_1")
TP = ("tp_0", "tp_1")
LANES = 128
COPY_ROWS = 256
AHEAD = 4
PLAN = (512, 512, 512, 512)
SEQ_ROWS = 16
ENDS_AT = 32
F32 = jnp.float32
BF16 = jnp.bfloat16


def lane_iota(shape):
    return lax.broadcasted_iota(jnp.int32, shape, len(shape) - 1)


def row_iota(shape):
    return lax.broadcasted_iota(jnp.int32, shape, 0)


def log_sigmoid(x):
    return jnp.minimum(x, 0.0) - jnp.log1p(jnp.exp(-jnp.abs(x)))


def key_activation(mixed):
    return (mixed * jax.nn.sigmoid(mixed) * KEY_DIM ** (-0.5)).astype(BF16)


def split(x):
    high = x.astype(BF16).astype(F32)
    middle = (x - high).astype(BF16).astype(F32)
    return [high, middle, x - high - middle]


def suffix_after(x):
    length = x.shape[-1]
    lanes = lane_iota(x.shape)

    def ahead(y, by):
        return jnp.where(lanes < length - by, pltpu.roll(y, length - by, y.ndim - 1), 0.0)

    total = ahead(x, 1)
    by = 1
    while by < length:
        total = total + ahead(total, by)
        by *= 2
    return total


def state_kernel(
    x_hbm, wk_hbm, wv_hbm, wi_hbm, wf_hbm, bias_hbm, taps_hbm, extra_hbm, out_ref,
    x_ref, w_ref, wi_ref, wf_ref, bias_ref, taps_ref, extra_ref, spread_ref, raw_ref, gate_ref, value_ref,
    x_sem, w_sem, small_sem,
):
    seqs, _, rows = extra_ref.shape
    total_rows, width = x_ref.shape
    owners = LANES // 8
    half = lane_iota((1, LANES)) < KEY_DIM

    small = [
        pltpu.make_async_copy(src, dst, small_sem.at[i])
        for i, (src, dst) in enumerate(
            [(wi_hbm, wi_ref), (wf_hbm, wf_ref), (bias_hbm, bias_ref), (taps_hbm, taps_ref), (extra_hbm, extra_ref)]
        )
    ]
    weights = [
        pltpu.make_async_copy(wk_hbm, w_ref.at[:, 0:LANES], w_sem.at[0]),
        pltpu.make_async_copy(wv_hbm, w_ref.at[:, 2 * LANES : 4 * LANES], w_sem.at[1]),
    ]
    blocks = [
        pltpu.make_async_copy(x_hbm.at[pl.ds(at, COPY_ROWS)], x_ref.at[pl.ds(at, COPY_ROWS)], x_sem.at[at // COPY_ROWS])
        for at in range(0, total_rows, COPY_ROWS)
    ]
    for copy in small + weights:
        copy.start()
    for copy in blocks[:AHEAD]:
        copy.start()
    for copy in small:
        copy.wait()

    pad = jnp.zeros((6, LANES), F32)
    tail = jnp.zeros((LANES - 16, LANES), F32)
    for c in range(width // LANES):
        cols = slice(c * LANES, (c + 1) * LANES)
        gates = jnp.concatenate([wi_ref[:, cols].astype(F32), pad, wf_ref[:, cols].astype(F32), pad, tail], axis=0)
        w_ref[cols, LANES : 2 * LANES] = gates.T.astype(BF16)
    spot = lax.broadcasted_iota(jnp.int32, spread_ref.shape, 0)
    goal = (spot // LANES) * 8 + spot % 8
    spread_ref[...] = jnp.where(goal == lane_iota(spread_ref.shape), 1.0, 0.0).astype(BF16)
    taps = taps_ref[...].astype(F32)
    bias = jnp.where(row_iota((2, 1)) == 0, bias_ref[:, 0:1], bias_ref[:, 1:2])
    for copy in weights:
        copy.wait()

    def project(start, count):
        at = slice(start, start + count)
        key_gate = jnp.dot(x_ref[at], w_ref[:, : 2 * LANES], preferred_element_type=F32)
        value = jnp.dot(x_ref[at], w_ref[:, 2 * LANES :], preferred_element_type=F32)
        raw_ref[at] = key_gate[:, :LANES].astype(BF16)
        gate_ref[at] = key_gate[:, LANES:]
        value_ref[at] = value.astype(BF16)

    def finish(s):
        own = slice(s * rows, (s + 1) * rows)
        values = value_ref[own]
        raw = raw_ref[own].astype(F32)
        gates = gate_ref[own].T
        input_pre = gates[0:2].astype(BF16).astype(F32)
        forget_pre = gates[8:10].astype(BF16).astype(F32)
        log_forget = log_sigmoid(forget_pre + bias) + extra_ref[s]
        gate_log = input_pre + suffix_after(log_forget)
        peak = jnp.max(gate_log, axis=1, keepdims=True)
        seg_total = jnp.sum(log_forget, axis=1, keepdims=True)
        scale = jnp.exp(gate_log - peak)

        before = pltpu.roll(raw, 1, 0)
        after = pltpu.roll(raw, rows - 1, 0)
        mixed = taps[0:1] * before + taps[1:2] * raw + taps[2:3] * after
        place = row_iota((rows, 1))
        inner = (place > 0) & (place < rows - 1)
        key_rows = jnp.where(inner, key_activation(mixed).astype(F32), 0.0)
        key_t = key_rows.T
        scaled_t = jnp.concatenate([key_t[:KEY_DIM] * scale[0:1], key_t[KEY_DIM:] * scale[1:2]], axis=0)
        memory = jnp.dot(scaled_t.astype(BF16), values, preferred_element_type=F32)
        memory = jnp.concatenate([memory[:KEY_DIM, :LANES], memory[KEY_DIM:, LANES:]], axis=0).T

        scale_parts = split(scale)
        pieces = jnp.concatenate(scale_parts + [jnp.zeros_like(scale)], axis=0).astype(BF16)
        norm = jnp.dot(pieces, key_rows.astype(BF16), preferred_element_type=F32)
        norm = jnp.where(half, norm[0:1] + norm[2:3] + norm[4:5], norm[1:2] + norm[3:4] + norm[5:6])

        ends = []
        for at in (0, rows - 1):
            for h in range(2):
                row = values[at : at + 1, h * LANES : (h + 1) * LANES].astype(F32)
                ends.append(row * scale[h : h + 1, at : at + 1])
        ends = jnp.concatenate(ends, axis=1)
        spot = lax.broadcasted_iota(jnp.int32, (owners, ends.shape[1]), 1)
        mine = (spot % LANES) // 8 == row_iota((owners, 1))
        picked = jnp.where(mine, ends, 0.0).astype(BF16)
        by_owner = jnp.dot(picked, spread_ref[...], preferred_element_type=F32)
        lane = lane_iota((1, LANES))
        ends_row = jnp.zeros((1, LANES), F32)
        stats_row = jnp.zeros((1, LANES), F32)
        for i, part in enumerate(scale_parts[:2]):
            for p, at in enumerate((0, rows - 1)):
                for h in range(2):
                    ends_row = jnp.where(lane == ENDS_AT + 4 * i + 2 * p + h, part[h : h + 1, at : at + 1], ends_row)
        for i, part in enumerate(split(peak) + split(seg_total)):
            for h in range(2):
                stats_row = jnp.where(lane == 2 * i + h, part[h : h + 1], stats_row)
        shared = jnp.concatenate([raw[0:2], raw[rows - 2 : rows]] + split(norm)[:2] + [ends_row, stats_row], axis=0)
        by_owner = jnp.where(row_iota((8, LANES))[None] == 6, by_owner[:, None, :], 0.0)
        block = jnp.concatenate([memory.reshape(owners, 8, LANES), shared[None] + by_owner], axis=1)
        out_ref[:, s * SEQ_ROWS : (s + 1) * SEQ_ROWS, :] = block.astype(BF16)

    done = 0
    finished = 0
    for count in PLAN:
        for i in range(done // COPY_ROWS, (done + count) // COPY_ROWS):
            blocks[i].wait()
            if i + AHEAD < len(blocks):
                blocks[i + AHEAD].start()
        project(done, count)
        ready = done // rows
        for s in range(finished, ready):
            finish(s)
        finished = ready
        done += count
    for s in range(finished, seqs):
        finish(s)


def prompt_states(prompt, key_weight, value_weight, input_gate_t, forget_gate_t, forget_bias, key_taps, extra_t):
    seqs, rows, width = prompt.shape
    owners = LANES // 8
    return pl.pallas_call(
        state_kernel,
        in_specs=[pl.BlockSpec(memory_space=pltpu.HBM)] * 8,
        out_specs=pl.BlockSpec(memory_space=pltpu.VMEM),
        out_shape=jax.ShapeDtypeStruct((owners, seqs * SEQ_ROWS, LANES), BF16),
        scratch_shapes=[
            pltpu.VMEM((seqs * rows, width), BF16),
            pltpu.VMEM((width, 4 * LANES), BF16),
            pltpu.VMEM(input_gate_t.shape, BF16),
            pltpu.VMEM(forget_gate_t.shape, BF16),
            pltpu.VMEM(forget_bias.shape, F32),
            pltpu.VMEM(key_taps.shape, BF16),
            pltpu.VMEM(extra_t.shape, F32),
            pltpu.VMEM((4 * LANES, LANES), BF16),
            pltpu.VMEM((seqs * rows, LANES), BF16),
            pltpu.VMEM((seqs * rows, LANES), F32),
            pltpu.VMEM((seqs * rows, 2 * LANES), BF16),
            pltpu.SemaphoreType.DMA((seqs * rows // COPY_ROWS,)),
            pltpu.SemaphoreType.DMA((2,)),
            pltpu.SemaphoreType.DMA((5,)),
        ],
        compiler_params=pltpu.CompilerParams(vmem_limit_bytes=60 * 1024 * 1024),
        name="prompt_states",
    )(prompt.reshape(seqs * rows, width), key_weight, value_weight, input_gate_t, forget_gate_t, forget_bias, key_taps, extra_t)


def paired(ref, s):
    rows = ref[s].astype(F32)
    return jnp.concatenate([rows[0:1], rows[1:2]], axis=1)


def read_kernel(
    index_ref, forget_ref, gate_ref, parts_ref, taps_ref, query_ref, key_ref, value_ref, weight_ref,
    memory_out, norm_out, peak_out, sent_out,
):
    devices = parts_ref.shape[0]
    seqs = query_ref.shape[0]
    half = lane_iota((1, LANES)) < KEY_DIM
    heads = jnp.where(half == (row_iota((2, LANES)) == 0), 1.0, 0.0).astype(BF16)
    device = row_iota((devices, 1))
    taps = taps_ref[...].astype(F32)
    contract = (((0,), (0,)), ((), ()))
    down = lambda y, by: jnp.where(device < devices - by, pltpu.roll(y, devices - by, 0), 0.0)
    reads = [jnp.zeros((8, LANES), F32), jnp.zeros((8, LANES), F32)]
    peaks = jnp.zeros((2, seqs), F32)
    for s in range(seqs):
        parts = parts_ref[:, s * SEQ_ROWS : (s + 1) * SEQ_ROWS, :].astype(F32)
        row = lambda r: parts[:, 8 + r, :]
        stats = row(7)

        def joined(first):
            ones = [stats[:, first + 2 * i : first + 2 * i + 1] for i in range(3)]
            twos = [stats[:, first + 2 * i + 1 : first + 2 * i + 2] for i in range(3)]
            return jnp.where(half, ones[0] + ones[1] + ones[2], twos[0] + twos[1] + twos[2])

        later = down(joined(6), 1)
        for by in (1, 2, 4, 8):
            later = later + down(later, by)
        level = joined(0) + later
        peak = jnp.max(level, axis=0, keepdims=True)
        factor = jnp.exp(level - peak)
        before = jnp.where(device > 0, pltpu.roll(row(3), 1, 0), 0.0)
        first = key_activation(taps[0:1] * before + taps[1:2] * row(0) + taps[2:3] * row(1)).astype(F32)
        last = key_activation(taps[0:1] * row(2) + taps[1:2] * row(3) + taps[2:3] * down(row(0), 1)).astype(F32)
        ends = row(6)
        at_first, at_last = (
            lax.dot_general(ends, rows * factor, contract, precision=lax.Precision.HIGHEST, preferred_element_type=F32)
            for rows in (first, last)
        )
        edge = jnp.where(half, at_first[0:8] + at_last[16:24], at_first[8:16] + at_last[24:32])
        scaled = at_first[32:33] + at_first[36:37] + at_last[34:35] + at_last[38:39]
        scaled_two = at_first[33:34] + at_first[37:38] + at_last[35:36] + at_last[39:40]
        norm_edge = jnp.where(half, scaled, scaled_two)
        memory = edge + jnp.sum(parts[:, 0:8, :] * factor[:, None, :], axis=0)
        norm = norm_edge + jnp.sum((row(4) + row(5)) * factor, axis=0, keepdims=True)
        memory_bf = memory.astype(BF16)
        memory_out[s, 0] = memory_bf[:, :KEY_DIM]
        memory_out[s, 1] = memory_bf[:, KEY_DIM:]
        own = pltpu.roll(norm, LANES - index_ref[0] * 4, 1)
        norm_out[s, 0:1, :] = own[:, 0:4].astype(BF16)
        norm_out[s, 1:2, :] = own[:, KEY_DIM : KEY_DIM + 4].astype(BF16)

        forget = log_sigmoid(jnp.where(half, forget_ref[0, s], forget_ref[1, s]))
        gate = jnp.where(half, gate_ref[0, s], gate_ref[1, s])
        new_peak = jnp.maximum(forget + peak, gate)
        old_scale = jnp.exp(forget + peak - new_peak)
        new_scale = jnp.exp(gate - new_peak)
        query = paired(query_ref, s)
        new_key = new_scale * paired(key_ref, s)
        new_value = lax.dot_general(value_ref[s], heads, contract, preferred_element_type=F32)
        numer = query * (old_scale * memory + new_key * new_value)
        denom = query * (old_scale * norm + new_key)
        spot = lane_iota((8, LANES))
        for h in range(2):
            side = half if h == 0 else jnp.logical_not(half)
            top = jnp.sum(jnp.where(side, numer, 0.0), axis=1, keepdims=True)
            bottom = jnp.sum(jnp.where(side, denom, 0.0), axis=1, keepdims=True)
            read = top / jnp.maximum(jnp.abs(bottom), 1.0)
            reads[h] = jnp.where((spot & 3) == s, read, reads[h])
            mark = (lane_iota(peaks.shape) == s) & (row_iota(peaks.shape) == h)
            peaks = jnp.where(mark, peak[:, h * KEY_DIM : h * KEY_DIM + 1], peaks)
    peak_out[...] = peaks
    read_rows = jnp.concatenate(reads, axis=0).T[0:8].astype(BF16)
    partial = jnp.dot(read_rows, weight_ref[...], preferred_element_type=F32)
    sub = row_iota((8, LANES))
    block = lane_iota((8, LANES)) // 32
    for m in range(partial.shape[1] // (2 * LANES)):
        low = partial[:, 2 * m * LANES : (2 * m + 1) * LANES]
        high = partial[:, (2 * m + 1) * LANES : (2 * m + 2) * LANES]
        both = jnp.where(sub < 4, low, high)
        out = jnp.zeros_like(both)
        for r in range(4):
            moved = pltpu.roll(both, 32 * r, 1) if r else both
            if r:
                near = pltpu.roll(moved, 8 - r, 0)
                wrap = pltpu.roll(moved, 4 - r, 0)
                moved = jnp.where((sub & 3) + r < 4, near, wrap)
            out = jnp.where(block == (((sub & 3) + r) & 3), moved, out)
        sent_out[8 * m : 8 * m + 8, :] = out


def first_read(index, forget, gate, parts, taps, query, key, value, weight):
    seqs = query.shape[0]
    vmem = pl.BlockSpec(memory_space=pltpu.VMEM)
    smem = pl.BlockSpec(memory_space=pltpu.SMEM)
    devices_all = weight.shape[1] // 32
    return pl.pallas_call(
        read_kernel,
        in_specs=[smem, smem, smem] + [vmem] * 6,
        out_specs=[vmem] * 4,
        out_shape=[
            jax.ShapeDtypeStruct((seqs, 2, 8, KEY_DIM), BF16),
            jax.ShapeDtypeStruct((seqs, 2, 4), BF16),
            jax.ShapeDtypeStruct((2, seqs), F32),
            jax.ShapeDtypeStruct((devices_all, LANES), F32),
        ],
        compiler_params=pltpu.CompilerParams(vmem_limit_bytes=32 * 1024 * 1024),
        name="first_read",
    )(index, forget, gate, parts, taps, query, key, value, weight)


def sum_kernel(parts_ref, out_ref):
    total = jnp.sum(parts_ref[...], axis=0, keepdims=True)
    for s in range(out_ref.shape[0]):
        out_ref[s : s + 1, :] = total[:, 32 * s : 32 * s + 32].astype(BF16)


def sum_parts(parts, seqs):
    vmem = pl.BlockSpec(memory_space=pltpu.VMEM)
    return pl.pallas_call(
        sum_kernel,
        in_specs=[vmem],
        out_specs=vmem,
        out_shape=jax.ShapeDtypeStruct((seqs, 32), BF16),
        name="sum_parts",
    )(parts)


def body(
    prompt, key_weight, value_weight, input_gate_weight, forget_gate_weight, forget_bias, key_taps,
    extra_decay, new_query, new_key, new_value, new_input_gate, new_forget_gate, out_weight,
):
    seqs = prompt.shape[0]
    index = lax.axis_index(SP).reshape(1)
    parts = prompt_states(
        prompt, key_weight, value_weight, input_gate_weight.T, forget_gate_weight.T, forget_bias.reshape(1, -1),
        key_taps, extra_decay.transpose(0, 2, 1),
    )
    parts = lax.all_to_all(parts, SP, 0, 0, tiled=True)
    memory, norm, peak, sent = first_read(
        index, new_forget_gate.T, new_input_gate.T, parts, key_taps, new_query, new_key, new_value,
        out_weight.reshape(-1, out_weight.shape[2]),
    )
    got = lax.all_to_all(sent.reshape(-1, 1, LANES), SP_TP, 0, 0, tiled=True)
    read_out = sum_parts(got.reshape(-1, LANES), seqs)
    return memory.swapaxes(2, 3), norm, peak.T, read_out


def solution(mesh):
    torus = Mesh(mesh.devices.reshape(4, 4, 4, 2), ("sp_0", "sp_1", "tp_0", "tp_1"))
    in_specs = (
        P(None, SP, None), P(None, TP), P(None, TP), P(None, TP), P(None, TP), P(TP), P(None, TP),
        P(None, SP, TP), P(None, TP, None), P(None, TP, None), P(None, TP, SP), P(None, TP), P(None, TP),
        P(TP, SP, None),
    )
    out_specs = (P(None, TP, None, SP), P(None, TP, SP), P(None, TP), P(None, SP_TP))
    return jax.shard_map(body, mesh=torus, in_specs=in_specs, out_specs=out_specs, check_vma=False)
```

time: 64 us -> 53.3 us (0.83)
  local copies, waits for them, and re-layouts: 6.97 us -> 0.03 us
  waiting for transfers between devices: 9.75 us -> 7.54 us
  Pallas kernels: 20.5 us -> 19.4 us
    unnamed x30 -> x14, local copies, waits for them, and re-layouts: 6.52 us -> 0.03 us
    all_to_all x1, waiting for transfers between devices: 9.75 us -> 7.54 us  [body(): parts = lax.all_to_all(parts, SP, 0, 0, tiled=True)]
    pallas_call x1, Pallas kernels: 17 us -> 15.4 us  [prompt_states(): pl.pallas_call(state_kernel, in_specs=[pl.BlockSpec(memory_space=pltpu.HB...]
  transfers between devices with their start and end apart: 1 -> 1, of which waited for: 1 -> 1; matrix products, arithmetic and copies ran while one was open for 1% -> 0% of each run, Pallas kernels for 0% -> 0%
where the time goes in v2:
time: 53.3 us; the launch traced here: 53.1 us
  Pallas kernels  19.4 us (36%)
  blocking collectives  17 us (32%)
  starting transfers between devices  8.43 us (16%)
  waiting for transfers between devices  7.54 us (14%)
  between operations  0.75 us (1%)
    all_to_all x1, blocking collectives, body(): got = lax.all_to_all(sent.reshape(-1, 1, LANES), SP_TP, 0, 0, tiled=True)  17 us
    pallas_call x1, Pallas kernels, prompt_states(): pl.pallas_call(state_kernel, in_specs=[pl.BlockSpec(memory_space=pltpu.HB...  15.4 us
    all_to_all x1, starting transfers between devices, body(): parts = lax.all_to_all(parts, SP, 0, 0, tiled=True)  8.43 us
    all_to_all x1, waiting for transfers between devices, body(): parts = lax.all_to_all(parts, SP, 0, 0, tiled=True)  7.54 us
    pallas_call x1, Pallas kernels, first_read(): pl.pallas_call(read_kernel, in_specs=[smem, smem, smem] + [vmem] * 6, out...  2.49 us
    pallas_call x1, Pallas kernels, sum_parts(): pl.pallas_call(sum_kernel, in_specs=[vmem], out_specs=vmem, out_shape=jax...  1.5 us
  transfers between devices with their start and end apart: 1, of which 1 were waited for; matrix products, arithmetic and copies ran while one was open for 0% of the time, Pallas kernels for 0%

profile of v2, /device:TPU:1, one launch (start us, length us, event | category | flops | bytes accessed | tf_op | source)
XLA Modules:
  0.0 53.1 jit_solution(8096807061045152719)
XLA Ops:
  0.6 0.0 copy-start.1
  0.6 0.0 copy-start
  0.7 0.0 copy-start.5
  0.7 0.0 copy-start.6
  0.7 0.0 copy-start.4
  0.7 0.0 copy-start.3
  0.7 0.0 copy-start.2
  0.7 15.4 %prompt_states.1 = bf16[16,64,128]{2,1,0:T(8,128)(2,1)} custom-call(bf16[2048,4096]{1,0:T(8,128)(2,1)} %bitcast.19, bf16[4096,128]{1,0:T(8,128)(2,1)} %wk_hbm.1, bf16[4096,256]{1,0:T(8,128)(2,1)} %wv_hbm.1, bf16[2,4096]{1,0:T(2,128)(2,1)} %bitcast.21, bf16[2,4096]{1,0:T(2,128)(2,1)} %bitcast.22, f32[1,2]{1,0:T(1,128)} %bitcast.24, bf16[3,128]{1,0:T(4,128)(2,1)} %taps_ref.1, ...), custom_call_target="tpu_custom_call" | custom-call | tf_op jit(solution)/shard_map/prompt_states/pallas_call | solution.py:187
  16.1 8.4 %all-to-all-start = ((bf16[16,64,128]{2,1,0:T(8,128)(2,1)}), bf16[16,64,128]{2,1,0:T(8,128)(2,1)S(1)}, u32[]{:S(2)}, u32[]{:S(2)}) async-start(bf16[16,64,128]{2,1,0:T(8,128)(2,1)} %prompt_states.1), calls=%async_computation | async-start | bytes 524288 | tf_op jit(solution)/shard_map/all_to_all | solution.py:355
  24.5 7.5 %all-to-all-done.parts_ref = bf16[16,64,128]{2,1,0:T(8,128)(2,1)S(1)} async-done(((bf16[16,64,128]{2,1,0:T(8,128)(2,1)}), bf16[16,64,128]{2,1,0:T(8,128)(2,1)S(1)}, u32[]{:S(2)}, u32[]{:S(2)}) %all-to-all-start) | async-done | bytes 262176 | tf_op jit(solution)/shard_map/all_to_all | solution.py:355
  32.1 0.0 copy-done.1
  32.1 0.0 copy-done
  32.1 0.0 copy-done.5
  32.1 0.0 copy-done.6
  32.1 0.0 copy-done.4
  32.1 0.0 copy-done.3
  32.1 0.0 copy-done.2
  32.1 2.5 %first_read.1 = (bf16[4,2,8,64]{3,2,1,0:T(8,128)(2,1)}, bf16[4,2,4]{2,1,0:T(2,128)(2,1)}, f32[2,4]{1,0:T(2,128)}, f32[128,128]{1,0:T(8,128)S(1)}) custom-call(s32[1]{0:T(128)} %bitcast.index_ref, f32[2,4]{1,0:T(2,128)S(1)} %bitcast.17, f32[2,4]{1,0:T(2,128)S(1)} %bitcast.18, bf16[16,64,128]{2,1,0:T(8,128)(2,1)S(1)} %all-to-all-done.parts_ref, ...), custom_call_target="tpu_custom_call" | custom-call | tf_op jit(solution)/shard_map/first_read/pallas_call | solution.py:313
  34.6 17.0 %all_to_all.10 = f32[128,1,128]{2,1,0:T(1,128)} all-to-all(f32[128,1,128]{2,1,0:T(1,128)S(1)} %bitcast.16), channel_id=1, replica_groups=mesh['sp_0'=4,'sp_1'=4,'tp_0'=4,'tp_1'=2] {'sp_0','sp_1','tp_0','tp_1'}, dimensions={0} | all-to-all | bytes 131072 | tf_op jit(solution)/shard_map/all_to_all | solution.py:360
  51.6 1.5 %sum_parts.1 = bf16[4,32]{1,0:T(4,128)(2,1)} custom-call(f32[128,128]{1,0:T(8,128)} %bitcast.20), custom_call_target="tpu_custom_call" | custom-call | tf_op jit(solution)/shard_map/sum_parts/pallas_call | solution.py:336
Async XLA Ops:
  0.6 31.4 %copy-start.1 = (bf16[3,128]{1,0:T(4,128)(2,1)S(1)}, bf16[3,128]{1,0:T(4,128)(2,1)}, u32[]{:S(2)}) copy-start(bf16[3,128]{1,0:T(4,128)(2,1)} %taps_ref.1) | copy-start | bytes 2308
  0.6 31.4 %copy-start = (bf16[2,8,4096]{2,1,0:T(8,128)(2,1)S(1)}, bf16[2,8,4096]{2,1,0:T(8,128)(2,1)}, u32[]{:S(2)}) copy-start(bf16[2,8,4096]{2,1,0:T(8,128)(2,1)} %param.27) | copy-start | bytes 393220
  0.7 31.4 %copy-start.5 = (f32[4,2]{0,1:T(2,128)S(1)}, f32[4,2]{0,1:T(2,128)}, u32[]{:S(2)}) copy-start(f32[4,2]{0,1:T(2,128)} %param.26) | copy-start | bytes 100
  0.7 31.4 %copy-start.6 = (f32[4,2]{0,1:T(2,128)S(1)}, f32[4,2]{0,1:T(2,128)}, u32[]{:S(2)}) copy-start(f32[4,2]{0,1:T(2,128)} %param.25) | copy-start | bytes 100
  0.7 31.4 %copy-start.4 = (bf16[4,2,8]{2,1,0:T(2,128)(2,1)S(1)}, bf16[4,2,8]{2,1,0:T(2,128)(2,1)}, u32[]{:S(2)}) copy-start(bf16[4,2,8]{2,1,0:T(2,128)(2,1)} %value_ref.1) | copy-start | bytes 388
  0.7 31.4 %copy-start.3 = (bf16[4,2,64]{2,1,0:T(2,128)(2,1)S(1)}, bf16[4,2,64]{2,1,0:T(2,128)(2,1)}, u32[]{:S(2)}) copy-start(bf16[4,2,64]{2,1,0:T(2,128)(2,1)} %key_ref.1) | copy-start | bytes 3076
  0.7 31.4 %copy-start.2 = (bf16[4,2,64]{2,1,0:T(2,128)(2,1)S(1)}, bf16[4,2,64]{2,1,0:T(2,128)(2,1)}, u32[]{:S(2)}) copy-start(bf16[4,2,64]{2,1,0:T(2,128)(2,1)} %query_ref.1) | copy-start | bytes 3076
  16.1 16.0 %all-to-all-start = ((bf16[16,64,128]{2,1,0:T(8,128)(2,1)}), bf16[16,64,128]{2,1,0:T(8,128)(2,1)S(1)}, u32[]{:S(2)}, u32[]{:S(2)}) async-start(bf16[16,64,128]{2,1,0:T(8,128)(2,1)} %prompt_states.1), calls=%async_computation | async-start | bytes 524288 | tf_op jit(solution)/shard_map/all_to_all | solution.py:355

commit v3 on v2

--- a/solution.py
+++ b/solution.py
@@ -12,8 +12,9 @@
 TP = ("tp_0", "tp_1")
 LANES = 128
 COPY_ROWS = 256
-AHEAD = 4
-PLAN = (512, 512, 512, 512)
+FIRST = 1
+AHEAD = 2
+PLAN = (256, 512, 512, 512, 256)
 SEQ_ROWS = 16
 ENDS_AT = 32
 F32 = jnp.float32
@@ -81,9 +82,7 @@
         pltpu.make_async_copy(x_hbm.at[pl.ds(at, COPY_ROWS)], x_ref.at[pl.ds(at, COPY_ROWS)], x_sem.at[at // COPY_ROWS])
         for at in range(0, total_rows, COPY_ROWS)
     ]
-    for copy in small + weights:
-        copy.start()
-    for copy in blocks[:AHEAD]:
+    for copy in small + weights[:1] + blocks[:FIRST] + weights[1:] + blocks[FIRST:AHEAD]:
         copy.start()
     for copy in small:
         copy.wait()
@@ -99,12 +98,13 @@
     spread_ref[...] = jnp.where(goal == lane_iota(spread_ref.shape), 1.0, 0.0).astype(BF16)
     taps = taps_ref[...].astype(F32)
     bias = jnp.where(row_iota((2, 1)) == 0, bias_ref[:, 0:1], bias_ref[:, 1:2])
-    for copy in weights:
-        copy.wait()
+    weights[0].wait()
 
     def project(start, count):
         at = slice(start, start + count)
         key_gate = jnp.dot(x_ref[at], w_ref[:, : 2 * LANES], preferred_element_type=F32)
+        if start == 0:
+            weights[1].wait()
         value = jnp.dot(x_ref[at], w_ref[:, 2 * LANES :], preferred_element_type=F32)
         raw_ref[at] = key_gate[:, :LANES].astype(BF16)
         gate_ref[at] = key_gate[:, LANES:]
@@ -188,7 +188,7 @@
         state_kernel,
         in_specs=[pl.BlockSpec(memory_space=pltpu.HBM)] * 8,
         out_specs=pl.BlockSpec(memory_space=pltpu.VMEM),
-        out_shape=jax.ShapeDtypeStruct((owners, seqs * SEQ_ROWS, LANES), BF16),
+        out_shape=pltpu.VMEM((owners, seqs * SEQ_ROWS, LANES), BF16),
         scratch_shapes=[
             pltpu.VMEM((seqs * rows, width), BF16),
             pltpu.VMEM((width, 4 * LANES), BF16),
@@ -338,6 +338,7 @@
         in_specs=[vmem],
         out_specs=vmem,
         out_shape=jax.ShapeDtypeStruct((seqs, 32), BF16),
+        compiler_params=pltpu.CompilerParams(vmem_limit_bytes=1024 * 1024),
         name="sum_parts",
     )(parts)
 
@@ -352,6 +353,7 @@
         prompt, key_weight, value_weight, input_gate_weight.T, forget_gate_weight.T, forget_bias.reshape(1, -1),
         key_taps, extra_decay.transpose(0, 2, 1),
     )
+    parts, index = lax.optimization_barrier((parts, index))
     parts = lax.all_to_all(parts, SP, 0, 0, tiled=True)
     memory, norm, peak, sent = first_read(
         index, new_forget_gate.T, new_input_gate.T, parts, key_taps, new_query, new_key, new_value,

time: 53.3 us -> 51 us (0.957)
  blocking collectives: 17 us -> 32.5 us
  starting transfers between devices: 8.43 us -> 0 us
  waiting for transfers between devices: 7.54 us -> 0 us
  Pallas kernels: 19.4 us -> 17.5 us
    all_to_all x0 -> x1, blocking collectives: none -> 15.8 us  [body(): parts = lax.all_to_all(parts, SP, 0, 0, tiled=True)]
    all_to_all x1 -> x0, starting transfers between devices: 8.43 us -> none  [body(): parts = lax.all_to_all(parts, SP, 0, 0, tiled=True)]
    all_to_all x1 -> x0, waiting for transfers between devices: 7.54 us -> none  [body(): parts = lax.all_to_all(parts, SP, 0, 0, tiled=True)]
    pallas_call x1, Pallas kernels: 15.4 us -> 14.4 us  [prompt_states(): pl.pallas_call(state_kernel, in_specs=[pl.BlockSpec(memory_space=pltpu.HB...]
    pallas_call x1, Pallas kernels: 1.5 us -> 0.66 us  [sum_parts(): pl.pallas_call(sum_kernel, in_specs=[vmem], out_specs=vmem, out_shape=jax...]
  transfers between devices with their start and end apart: 1 -> 0, of which waited for: 1 -> 0; matrix products, arithmetic and copies ran while one was open for 0% -> 0% of each run, Pallas kernels for 0% -> 0%
where the time goes in v3:
time: 51 us; the launch traced here: 50.8 us
  blocking collectives  32.5 us (64%)
  Pallas kernels  17.5 us (34%)
  between operations  0.74 us (1%)
    all_to_all x1, blocking collectives, body(): got = lax.all_to_all(sent.reshape(-1, 1, LANES), SP_TP, 0, 0, tiled=True)  16.7 us
    all_to_all x1, blocking collectives, body(): parts = lax.all_to_all(parts, SP, 0, 0, tiled=True)  15.8 us
    pallas_call x1, Pallas kernels, prompt_states(): pl.pallas_call(state_kernel, in_specs=[pl.BlockSpec(memory_space=pltpu.HB...  14.4 us
    pallas_call x1, Pallas kernels, first_read(): pl.pallas_call(read_kernel, in_specs=[smem, smem, smem] + [vmem] * 6, out...  2.48 us

profile of v3, /device:TPU:1, one launch (start us, length us, event | category | flops | bytes accessed | tf_op | source)
XLA Modules:
  0.0 50.8 jit_solution(10556919470788638114)
XLA Ops:
  0.6 0.0 copy-start.1
  0.6 0.0 copy-start
  0.7 0.0 copy-start.5
  0.7 0.0 copy-start.6
  0.7 0.0 copy-start.4
  0.7 0.0 copy-start.3
  0.7 0.0 copy-start.2
  0.7 14.4 %prompt_states.1 = bf16[16,64,128]{2,1,0:T(8,128)(2,1)S(1)} custom-call(bf16[2048,4096]{1,0:T(8,128)(2,1)} %bitcast.20, bf16[4096,128]{1,0:T(8,128)(2,1)} %wk_hbm.1, bf16[4096,256]{1,0:T(8,128)(2,1)} %wv_hbm.1, bf16[2,4096]{1,0:T(2,128)(2,1)} %bitcast.21, bf16[2,4096]{1,0:T(2,128)(2,1)} %bitcast.22, f32[1,2]{1,0:T(1,128)} %bitcast.24, ...), custom_call_target="tpu_custom_call" | custom-call | tf_op jit(solution)/shard_map/prompt_states/pallas_call | solution.py:187
  15.1 15.8 %all_to_all.10.parts_ref = bf16[16,64,128]{2,1,0:T(8,128)(2,1)S(1)} all-to-all(bf16[16,64,128]{2,1,0:T(8,128)(2,1)S(1)} %prompt_states.1), channel_id=1, replica_groups=mesh['sp_0'=4,'sp_1'=4,'tp_0'=4,'tp_1'=2] {'sp_0','sp_1'}, dimensions={0} | all-to-all | bytes 524288 | tf_op jit(solution)/shard_map/all_to_all | solution.py:357
  30.9 0.0 copy-done.1
  30.9 0.0 copy-done
  30.9 0.0 copy-done.5
  30.9 0.0 copy-done.6
  30.9 0.0 copy-done.4
  30.9 0.0 copy-done.3
  30.9 0.0 copy-done.2
  30.9 2.5 %first_read.1 = (bf16[4,2,8,64]{3,2,1,0:T(8,128)(2,1)}, bf16[4,2,4]{2,1,0:T(2,128)(2,1)}, f32[2,4]{1,0:T(2,128)}, f32[128,128]{1,0:T(8,128)S(1)}) custom-call(s32[1]{0:T(128)} %bitcast.5.index_ref, f32[2,4]{1,0:T(2,128)S(1)} %bitcast.18, f32[2,4]{1,0:T(2,128)S(1)} %bitcast.19, bf16[16,64,128]{2,1,0:T(8,128)(2,1)S(1)} %all_to_all.10.parts_ref, ...), custom_call_target="tpu_custom_call" | custom-call | tf_op jit(solution)/shard_map/first_read/pallas_call | solution.py:313
  33.4 16.7 %all_to_all.11 = f32[128,1,128]{2,1,0:T(1,128)S(1)} all-to-all(f32[128,1,128]{2,1,0:T(1,128)S(1)} %bitcast.17), channel_id=1, replica_groups=mesh['sp_0'=4,'sp_1'=4,'tp_0'=4,'tp_1'=2] {'sp_0','sp_1','tp_0','tp_1'}, dimensions={0} | all-to-all | bytes 131072 | tf_op jit(solution)/shard_map/all_to_all | solution.py:362
  50.1 0.7 %sum_parts.1 = bf16[4,32]{1,0:T(4,128)(2,1)} custom-call(f32[128,128]{1,0:T(8,128)S(1)} %bitcast.15), custom_call_target="tpu_custom_call" | custom-call | tf_op jit(solution)/shard_map/sum_parts/pallas_call | solution.py:336
Async XLA Ops:
  0.6 30.2 %copy-start.1 = (bf16[3,128]{1,0:T(4,128)(2,1)S(1)}, bf16[3,128]{1,0:T(4,128)(2,1)}, u32[]{:S(2)}) copy-start(bf16[3,128]{1,0:T(4,128)(2,1)} %taps_ref.1) | copy-start | bytes 2308
  0.6 30.2 %copy-start = (bf16[2,8,4096]{2,1,0:T(8,128)(2,1)S(1)}, bf16[2,8,4096]{2,1,0:T(8,128)(2,1)}, u32[]{:S(2)}) copy-start(bf16[2,8,4096]{2,1,0:T(8,128)(2,1)} %param.27) | copy-start | bytes 393220
  0.7 30.2 %copy-start.5 = (f32[4,2]{0,1:T(2,128)S(1)}, f32[4,2]{0,1:T(2,128)}, u32[]{:S(2)}) copy-start(f32[4,2]{0,1:T(2,128)} %param.26) | copy-start | bytes 100
  0.7 30.2 %copy-start.6 = (f32[4,2]{0,1:T(2,128)S(1)}, f32[4,2]{0,1:T(2,128)}, u32[]{:S(2)}) copy-start(f32[4,2]{0,1:T(2,128)} %param.25) | copy-start | bytes 100
  0.7 30.2 %copy-start.4 = (bf16[4,2,8]{2,1,0:T(2,128)(2,1)S(1)}, bf16[4,2,8]{2,1,0:T(2,128)(2,1)}, u32[]{:S(2)}) copy-start(bf16[4,2,8]{2,1,0:T(2,128)(2,1)} %value_ref.1) | copy-start | bytes 388
  0.7 30.2 %copy-start.3 = (bf16[4,2,64]{2,1,0:T(2,128)(2,1)S(1)}, bf16[4,2,64]{2,1,0:T(2,128)(2,1)}, u32[]{:S(2)}) copy-start(bf16[4,2,64]{2,1,0:T(2,128)(2,1)} %key_ref.1) | copy-start | bytes 3076
  0.7 30.2 %copy-start.2 = (bf16[4,2,64]{2,1,0:T(2,128)(2,1)S(1)}, bf16[4,2,64]{2,1,0:T(2,128)(2,1)}, u32[]{:S(2)}) copy-start(bf16[4,2,64]{2,1,0:T(2,128)(2,1)} %query_ref.1) | copy-start | bytes 3076

commit v4 on v3

--- a/solution.py
+++ b/solution.py
@@ -12,8 +12,7 @@
 TP = ("tp_0", "tp_1")
 LANES = 128
 COPY_ROWS = 256
-FIRST = 1
-AHEAD = 2
+ISSUED = (3, 5, 7, 8, 8)
 PLAN = (256, 512, 512, 512, 256)
 SEQ_ROWS = 16
 ENDS_AT = 32
@@ -82,7 +81,7 @@
         pltpu.make_async_copy(x_hbm.at[pl.ds(at, COPY_ROWS)], x_ref.at[pl.ds(at, COPY_ROWS)], x_sem.at[at // COPY_ROWS])
         for at in range(0, total_rows, COPY_ROWS)
     ]
-    for copy in small + weights[:1] + blocks[:FIRST] + weights[1:] + blocks[FIRST:AHEAD]:
+    for copy in small + weights[:1] + blocks[:1]:
         copy.start()
     for copy in small:
         copy.wait()
@@ -99,6 +98,7 @@
     taps = taps_ref[...].astype(F32)
     bias = jnp.where(row_iota((2, 1)) == 0, bias_ref[:, 0:1], bias_ref[:, 1:2])
     weights[0].wait()
+    weights[1].start()
 
     def project(start, count):
         at = slice(start, start + count)
@@ -110,7 +110,7 @@
         gate_ref[at] = key_gate[:, LANES:]
         value_ref[at] = value.astype(BF16)
 
-    def finish(s):
+    def prepare(s):
         own = slice(s * rows, (s + 1) * rows)
         values = value_ref[own]
         raw = raw_ref[own].astype(F32)
@@ -131,14 +131,8 @@
         key_rows = jnp.where(inner, key_activation(mixed).astype(F32), 0.0)
         key_t = key_rows.T
         scaled_t = jnp.concatenate([key_t[:KEY_DIM] * scale[0:1], key_t[KEY_DIM:] * scale[1:2]], axis=0)
-        memory = jnp.dot(scaled_t.astype(BF16), values, preferred_element_type=F32)
-        memory = jnp.concatenate([memory[:KEY_DIM, :LANES], memory[KEY_DIM:, LANES:]], axis=0).T
-
         scale_parts = split(scale)
         pieces = jnp.concatenate(scale_parts + [jnp.zeros_like(scale)], axis=0).astype(BF16)
-        norm = jnp.dot(pieces, key_rows.astype(BF16), preferred_element_type=F32)
-        norm = jnp.where(half, norm[0:1] + norm[2:3] + norm[4:5], norm[1:2] + norm[3:4] + norm[5:6])
-
         ends = []
         for at in (0, rows - 1):
             for h in range(2):
@@ -148,7 +142,6 @@
         spot = lax.broadcasted_iota(jnp.int32, (owners, ends.shape[1]), 1)
         mine = (spot % LANES) // 8 == row_iota((owners, 1))
         picked = jnp.where(mine, ends, 0.0).astype(BF16)
-        by_owner = jnp.dot(picked, spread_ref[...], preferred_element_type=F32)
         lane = lane_iota((1, LANES))
         ends_row = jnp.zeros((1, LANES), F32)
         stats_row = jnp.zeros((1, LANES), F32)
@@ -159,26 +152,43 @@
         for i, part in enumerate(split(peak) + split(seg_total)):
             for h in range(2):
                 stats_row = jnp.where(lane == 2 * i + h, part[h : h + 1], stats_row)
-        shared = jnp.concatenate([raw[0:2], raw[rows - 2 : rows]] + split(norm)[:2] + [ends_row, stats_row], axis=0)
+        raw_rows = jnp.concatenate([raw[0:2], raw[rows - 2 : rows]], axis=0)
+        return scaled_t.astype(BF16), pieces, key_rows.astype(BF16), picked, raw_rows, ends_row, stats_row
+
+    def finish(s, prepared):
+        scaled_t, pieces, key_rows, picked, raw_rows, ends_row, stats_row = prepared
+        values = value_ref[s * rows : (s + 1) * rows]
+        memory = jnp.dot(scaled_t, values, preferred_element_type=F32)
+        memory = jnp.concatenate([memory[:KEY_DIM, :LANES], memory[KEY_DIM:, LANES:]], axis=0).T
+        norm = jnp.dot(pieces, key_rows, preferred_element_type=F32)
+        norm = jnp.where(half, norm[0:1] + norm[2:3] + norm[4:5], norm[1:2] + norm[3:4] + norm[5:6])
+        by_owner = jnp.dot(picked, spread_ref[...], preferred_element_type=F32)
+        shared = jnp.concatenate([raw_rows] + split(norm)[:2] + [ends_row, stats_row], axis=0)
         by_owner = jnp.where(row_iota((8, LANES))[None] == 6, by_owner[:, None, :], 0.0)
         block = jnp.concatenate([memory.reshape(owners, 8, LANES), shared[None] + by_owner], axis=1)
         out_ref[:, s * SEQ_ROWS : (s + 1) * SEQ_ROWS, :] = block.astype(BF16)
 
     done = 0
     finished = 0
-    for count in PLAN:
+    prepared = {}
+    sent = 1
+    for step, count in enumerate(PLAN):
         for i in range(done // COPY_ROWS, (done + count) // COPY_ROWS):
             blocks[i].wait()
-            if i + AHEAD < len(blocks):
-                blocks[i + AHEAD].start()
+        for i in range(sent, min(len(blocks), ISSUED[step])):
+            blocks[i].start()
+        sent = max(sent, ISSUED[step])
+        for s in prepared:
+            finish(s, prepared[s])
         project(done, count)
         ready = done // rows
-        for s in range(finished, ready):
-            finish(s)
+        prepared = {s: prepare(s) for s in range(finished, ready)}
         finished = ready
         done += count
+    for s in prepared:
+        finish(s, prepared[s])
     for s in range(finished, seqs):
-        finish(s)
+        finish(s, prepare(s))
 
 
 def prompt_states(prompt, key_weight, value_weight, input_gate_t, forget_gate_t, forget_bias, key_taps, extra_t):
@@ -216,18 +226,22 @@
 
 
 def read_kernel(
-    index_ref, forget_ref, gate_ref, parts_ref, taps_ref, query_ref, key_ref, value_ref, weight_ref,
-    memory_out, norm_out, peak_out, sent_out,
+    forget_ref, gate_ref, parts_ref, taps_ref, query_ref, key_ref, value_ref, weight_ref,
+    memory_hbm, norm_hbm, peak_hbm, sent_out, memory_out, norm_out, peak_out, sems,
 ):
     devices = parts_ref.shape[0]
     seqs = query_ref.shape[0]
     half = lane_iota((1, LANES)) < KEY_DIM
     heads = jnp.where(half == (row_iota((2, LANES)) == 0), 1.0, 0.0).astype(BF16)
     device = row_iota((devices, 1))
+    lane = lane_iota((devices, LANES))
+    at_first = (lane < 16) | ((lane & 2) == 0) & (lane >= ENDS_AT)
     taps = taps_ref[...].astype(F32)
     contract = (((0,), (0,)), ((), ()))
     down = lambda y, by: jnp.where(device < devices - by, pltpu.roll(y, devices - by, 0), 0.0)
-    reads = [jnp.zeros((8, LANES), F32), jnp.zeros((8, LANES), F32)]
+    by_head = lambda ref, s: jnp.where(half, ref[0:1, s : s + 1], ref[1:2, s : s + 1])
+    own_first = LANES - lax.axis_index(SP) * 4
+    memories, norms, levels = [], [], []
     peaks = jnp.zeros((2, seqs), F32)
     for s in range(seqs):
         parts = parts_ref[:, s * SEQ_ROWS : (s + 1) * SEQ_ROWS, :].astype(F32)
@@ -249,25 +263,39 @@
         first = key_activation(taps[0:1] * before + taps[1:2] * row(0) + taps[2:3] * row(1)).astype(F32)
         last = key_activation(taps[0:1] * row(2) + taps[1:2] * row(3) + taps[2:3] * down(row(0), 1)).astype(F32)
         ends = row(6)
-        at_first, at_last = (
-            lax.dot_general(ends, rows * factor, contract, precision=lax.Precision.HIGHEST, preferred_element_type=F32)
-            for rows in (first, last)
-        )
-        edge = jnp.where(half, at_first[0:8] + at_last[16:24], at_first[8:16] + at_last[24:32])
-        scaled = at_first[32:33] + at_first[36:37] + at_last[34:35] + at_last[38:39]
-        scaled_two = at_first[33:34] + at_first[37:38] + at_last[35:36] + at_last[39:40]
-        norm_edge = jnp.where(half, scaled, scaled_two)
+        ends_first, ends_last = jnp.where(at_first, ends, 0.0), jnp.where(at_first, 0.0, ends)
+        left = jnp.concatenate([ends_first, ends_first, ends_last, ends_last], axis=0).astype(BF16)
+        right = jnp.concatenate(split(first * factor)[:2] + split(last * factor)[:2], axis=0).astype(BF16)
+        edges = lax.dot_general(left, right, contract, preferred_element_type=F32)
+        edge = jnp.where(half, edges[0:8] + edges[16:24], edges[8:16] + edges[24:32])
+        scaled = edges[32:33] + edges[34:35] + edges[36:37] + edges[38:39]
+        scaled_two = edges[33:34] + edges[35:36] + edges[37:38] + edges[39:40]
         memory = edge + jnp.sum(parts[:, 0:8, :] * factor[:, None, :], axis=0)
-        norm = norm_edge + jnp.sum((row(4) + row(5)) * factor, axis=0, keepdims=True)
+        norm = jnp.where(half, scaled, scaled_two) + jnp.sum((row(4) + row(5)) * factor, axis=0, keepdims=True)
         memory_bf = memory.astype(BF16)
         memory_out[s, 0] = memory_bf[:, :KEY_DIM]
         memory_out[s, 1] = memory_bf[:, KEY_DIM:]
-        own = pltpu.roll(norm, LANES - index_ref[0] * 4, 1)
+        own = pltpu.roll(norm, own_first, 1)
         norm_out[s, 0:1, :] = own[:, 0:4].astype(BF16)
         norm_out[s, 1:2, :] = own[:, KEY_DIM : KEY_DIM + 4].astype(BF16)
-
-        forget = log_sigmoid(jnp.where(half, forget_ref[0, s], forget_ref[1, s]))
-        gate = jnp.where(half, gate_ref[0, s], gate_ref[1, s])
+        for h in range(2):
+            mark = (lane_iota(peaks.shape) == s) & (row_iota(peaks.shape) == h)
+            peaks = jnp.where(mark, peak[:, h * KEY_DIM : h * KEY_DIM + 1], peaks)
+        memories.append(memory)
+        norms.append(norm)
+        levels.append(peak)
+    peak_out[...] = peaks
+    copies = [
+        pltpu.make_async_copy(src, dst, sems.at[i])
+        for i, (src, dst) in enumerate([(memory_out, memory_hbm), (norm_out, norm_hbm), (peak_out, peak_hbm)])
+    ]
+    for copy in copies:
+        copy.start()
+
+    reads = [jnp.zeros((8, LANES), F32), jnp.zeros((8, LANES), F32)]
+    for s, (memory, norm, peak) in enumerate(zip(memories, norms, levels)):
+        forget = log_sigmoid(by_head(forget_ref, s))
+        gate = by_head(gate_ref, s)
         new_peak = jnp.maximum(forget + peak, gate)
         old_scale = jnp.exp(forget + peak - new_peak)
         new_scale = jnp.exp(gate - new_peak)
@@ -283,9 +311,6 @@
             bottom = jnp.sum(jnp.where(side, denom, 0.0), axis=1, keepdims=True)
             read = top / jnp.maximum(jnp.abs(bottom), 1.0)
             reads[h] = jnp.where((spot & 3) == s, read, reads[h])
-            mark = (lane_iota(peaks.shape) == s) & (row_iota(peaks.shape) == h)
-            peaks = jnp.where(mark, peak[:, h * KEY_DIM : h * KEY_DIM + 1], peaks)
-    peak_out[...] = peaks
     read_rows = jnp.concatenate(reads, axis=0).T[0:8].astype(BF16)
     partial = jnp.dot(read_rows, weight_ref[...], preferred_element_type=F32)
     sub = row_iota((8, LANES))
@@ -303,26 +328,30 @@
                 moved = jnp.where((sub & 3) + r < 4, near, wrap)
             out = jnp.where(block == (((sub & 3) + r) & 3), moved, out)
         sent_out[8 * m : 8 * m + 8, :] = out
-
-
-def first_read(index, forget, gate, parts, taps, query, key, value, weight):
+    for copy in copies:
+        copy.wait()
+
+
+def first_read(forget, gate, parts, taps, query, key, value, weight):
     seqs = query.shape[0]
     vmem = pl.BlockSpec(memory_space=pltpu.VMEM)
-    smem = pl.BlockSpec(memory_space=pltpu.SMEM)
+    hbm = pl.BlockSpec(memory_space=pltpu.HBM)
     devices_all = weight.shape[1] // 32
+    memory, norm, peak = (((seqs, 2, 8, KEY_DIM), BF16), ((seqs, 2, 4), BF16), ((2, seqs), F32))
     return pl.pallas_call(
         read_kernel,
-        in_specs=[smem, smem, smem] + [vmem] * 6,
-        out_specs=[vmem] * 4,
+        in_specs=[vmem] * 8,
+        out_specs=[hbm] * 3 + [vmem],
         out_shape=[
-            jax.ShapeDtypeStruct((seqs, 2, 8, KEY_DIM), BF16),
-            jax.ShapeDtypeStruct((seqs, 2, 4), BF16),
-            jax.ShapeDtypeStruct((2, seqs), F32),
-            jax.ShapeDtypeStruct((devices_all, LANES), F32),
+            pltpu.HBM(*memory),
+            pltpu.HBM(*norm),
+            pltpu.HBM(*peak),
+            pltpu.VMEM((devices_all, LANES), F32),
         ],
+        scratch_shapes=[pltpu.VMEM(*memory), pltpu.VMEM(*norm), pltpu.VMEM(*peak), pltpu.SemaphoreType.DMA((3,))],
         compiler_params=pltpu.CompilerParams(vmem_limit_bytes=32 * 1024 * 1024),
         name="first_read",
-    )(index, forget, gate, parts, taps, query, key, value, weight)
+    )(forget, gate, parts, taps, query, key, value, weight)
 
 
 def sum_kernel(parts_ref, out_ref):
@@ -348,15 +377,13 @@
     extra_decay, new_query, new_key, new_value, new_input_gate, new_forget_gate, out_weight,
 ):
     seqs = prompt.shape[0]
-    index = lax.axis_index(SP).reshape(1)
     parts = prompt_states(
         prompt, key_weight, value_weight, input_gate_weight.T, forget_gate_weight.T, forget_bias.reshape(1, -1),
         key_taps, extra_decay.transpose(0, 2, 1),
     )
-    parts, index = lax.optimization_barrier((parts, index))
     parts = lax.all_to_all(parts, SP, 0, 0, tiled=True)
     memory, norm, peak, sent = first_read(
-        index, new_forget_gate.T, new_input_gate.T, parts, key_taps, new_query, new_key, new_value,
+        new_forget_gate.T, new_input_gate.T, parts, key_taps, new_query, new_key, new_value,
         out_weight.reshape(-1, out_weight.shape[2]),
     )
     got = lax.all_to_all(sent.reshape(-1, 1, LANES), SP_TP, 0, 0, tiled=True)

time: 51 us -> 50 us (0.980)
  Pallas kernels: 17.5 us -> 16.6 us
    pallas_call x1, Pallas kernels: 2.48 us -> 1.92 us  [first_read(): pl.pallas_call(read_kernel, in_specs=[vmem] * 8, out_specs=[hbm] * 3 + [v...]
where the time goes in v4:
time: 50 us; the launch traced here: 49.9 us
  blocking collectives  32.5 us (65%)
  Pallas kernels  16.6 us (33%)
  between operations  0.74 us (1%)
    all_to_all x1, blocking collectives, body(): got = lax.all_to_all(sent.reshape(-1, 1, LANES), SP_TP, 0, 0, tiled=True)  16.8 us
    all_to_all x1, blocking collectives, body(): parts = lax.all_to_all(parts, SP, 0, 0, tiled=True)  15.8 us
    pallas_call x1, Pallas kernels, prompt_states(): pl.pallas_call(state_kernel, in_specs=[pl.BlockSpec(memory_space=pltpu.HB...  14 us
    pallas_call x1, Pallas kernels, first_read(): pl.pallas_call(read_kernel, in_specs=[vmem] * 8, out_specs=[hbm] * 3 + [v...  1.92 us

profile of v4, /device:TPU:1, one launch (start us, length us, event | category | flops | bytes accessed | tf_op | source)
XLA Modules:
  0.0 49.9 jit_solution(2898184245787206674)
XLA Ops:
  0.6 0.0 copy-start.1
  0.6 0.0 copy-start
  0.7 0.0 copy-start.5
  0.7 0.0 copy-start.6
  0.7 0.0 copy-start.4
  0.7 0.0 copy-start.3
  0.7 0.0 copy-start.2
  0.7 14.0 %prompt_states.1 = bf16[16,64,128]{2,1,0:T(8,128)(2,1)S(1)} custom-call(bf16[2048,4096]{1,0:T(8,128)(2,1)} %bitcast.19, bf16[4096,128]{1,0:T(8,128)(2,1)} %wk_hbm.1, bf16[4096,256]{1,0:T(8,128)(2,1)} %wv_hbm.1, bf16[2,4096]{1,0:T(2,128)(2,1)} %bitcast.20, bf16[2,4096]{1,0:T(2,128)(2,1)} %bitcast.21, f32[1,2]{1,0:T(1,128)} %bitcast.23, ...), custom_call_target="tpu_custom_call" | custom-call | tf_op jit(solution)/shard_map/prompt_states/pallas_call | solution.py:197
  14.7 15.8 %all_to_all.10.parts_ref = bf16[16,64,128]{2,1,0:T(8,128)(2,1)S(1)} all-to-all(bf16[16,64,128]{2,1,0:T(8,128)(2,1)S(1)} %prompt_states.1), channel_id=1, replica_groups=mesh['sp_0'=4,'sp_1'=4,'tp_0'=4,'tp_1'=2] {'sp_0','sp_1'}, dimensions={0} | all-to-all | bytes 524288 | tf_op jit(solution)/shard_map/all_to_all | solution.py:384
  30.5 0.0 copy-done.1
  30.5 0.0 copy-done
  30.5 0.0 copy-done.5
  30.5 0.0 copy-done.6
  30.5 0.0 copy-done.4
  30.5 0.0 copy-done.3
  30.5 0.0 copy-done.2
  30.5 1.9 %first_read.1 = (bf16[4,2,8,64]{3,2,1,0:T(8,128)(2,1)}, bf16[4,2,4]{2,1,0:T(2,128)(2,1)}, f32[2,4]{1,0:T(2,128)}, f32[128,128]{1,0:T(8,128)S(1)}) custom-call(f32[2,4]{1,0:T(2,128)S(1)} %bitcast.17, f32[2,4]{1,0:T(2,128)S(1)} %bitcast.18, bf16[16,64,128]{2,1,0:T(8,128)(2,1)S(1)} %all_to_all.10.parts_ref, bf16[3,128]{1,0:T(4,128)(2,1)S(1)} %copy-done.1, ...), custom_call_target="tpu_custom_call" | custom-call | tf_op jit(solution)/shard_map/first_read/pallas_call | solution.py:341
  32.4 16.8 %all_to_all.11 = f32[128,1,128]{2,1,0:T(1,128)S(1)} all-to-all(f32[128,1,128]{2,1,0:T(1,128)S(1)} %bitcast.16), channel_id=1, replica_groups=mesh['sp_0'=4,'sp_1'=4,'tp_0'=4,'tp_1'=2] {'sp_0','sp_1','tp_0','tp_1'}, dimensions={0} | all-to-all | bytes 131072 | tf_op jit(solution)/shard_map/all_to_all | solution.py:389
  49.2 0.7 %sum_parts.1 = bf16[4,32]{1,0:T(4,128)(2,1)} custom-call(f32[128,128]{1,0:T(8,128)S(1)} %bitcast.14), custom_call_target="tpu_custom_call" | custom-call | tf_op jit(solution)/shard_map/sum_parts/pallas_call | solution.py:365
Async XLA Ops:
  0.6 29.8 %copy-start.1 = (bf16[3,128]{1,0:T(4,128)(2,1)S(1)}, bf16[3,128]{1,0:T(4,128)(2,1)}, u32[]{:S(2)}) copy-start(bf16[3,128]{1,0:T(4,128)(2,1)} %taps_ref.1) | copy-start | bytes 2308
  0.6 29.8 %copy-start = (bf16[2,8,4096]{2,1,0:T(8,128)(2,1)S(1)}, bf16[2,8,4096]{2,1,0:T(8,128)(2,1)}, u32[]{:S(2)}) copy-start(bf16[2,8,4096]{2,1,0:T(8,128)(2,1)} %param.27) | copy-start | bytes 393220
  0.7 29.8 %copy-start.5 = (f32[4,2]{0,1:T(2,128)S(1)}, f32[4,2]{0,1:T(2,128)}, u32[]{:S(2)}) copy-start(f32[4,2]{0,1:T(2,128)} %param.26) | copy-start | bytes 100
  0.7 29.8 %copy-start.6 = (f32[4,2]{0,1:T(2,128)S(1)}, f32[4,2]{0,1:T(2,128)}, u32[]{:S(2)}) copy-start(f32[4,2]{0,1:T(2,128)} %param.25) | copy-start | bytes 100
  0.7 29.8 %copy-start.4 = (bf16[4,2,8]{2,1,0:T(2,128)(2,1)S(1)}, bf16[4,2,8]{2,1,0:T(2,128)(2,1)}, u32[]{:S(2)}) copy-start(bf16[4,2,8]{2,1,0:T(2,128)(2,1)} %value_ref.1) | copy-start | bytes 388
  0.7 29.8 %copy-start.3 = (bf16[4,2,64]{2,1,0:T(2,128)(2,1)S(1)}, bf16[4,2,64]{2,1,0:T(2,128)(2,1)}, u32[]{:S(2)}) copy-start(bf16[4,2,64]{2,1,0:T(2,128)(2,1)} %key_ref.1) | copy-start | bytes 3076
  0.7 29.8 %copy-start.2 = (bf16[4,2,64]{2,1,0:T(2,128)(2,1)S(1)}, bf16[4,2,64]{2,1,0:T(2,128)(2,1)}, u32[]{:S(2)}) copy-start(bf16[4,2,64]{2,1,0:T(2,128)(2,1)} %query_ref.1) | copy-start | bytes 3076

commit v5 on v4

--- a/solution.py
+++ b/solution.py
@@ -85,6 +85,7 @@
         copy.start()
     for copy in small:
         copy.wait()
+    weights[1].start()
 
     pad = jnp.zeros((6, LANES), F32)
     tail = jnp.zeros((LANES - 16, LANES), F32)
@@ -98,7 +99,6 @@
     taps = taps_ref[...].astype(F32)
     bias = jnp.where(row_iota((2, 1)) == 0, bias_ref[:, 0:1], bias_ref[:, 1:2])
     weights[0].wait()
-    weights[1].start()
 
     def project(start, count):
         at = slice(start, start + count)

time: 50 us -> 50 us (level)
  no operation moved by 1% of the time
where the time goes in v5:
time: 50 us; the launch traced here: 49.9 us
  blocking collectives  32.5 us (65%)
  Pallas kernels  16.6 us (33%)
  between operations  0.74 us (1%)
    all_to_all x1, blocking collectives, body(): got = lax.all_to_all(sent.reshape(-1, 1, LANES), SP_TP, 0, 0, tiled=True)  16.8 us
    all_to_all x1, blocking collectives, body(): parts = lax.all_to_all(parts, SP, 0, 0, tiled=True)  15.8 us
    pallas_call x1, Pallas kernels, prompt_states(): pl.pallas_call(state_kernel, in_specs=[pl.BlockSpec(memory_space=pltpu.HB...  14 us
    pallas_call x1, Pallas kernels, first_read(): pl.pallas_call(read_kernel, in_specs=[vmem] * 8, out_specs=[hbm] * 3 + [v...  1.92 us

profile of v5, /device:TPU:1, one launch (start us, length us, event | category | flops | bytes accessed | tf_op | source)
XLA Modules:
  0.0 49.9 jit_solution(1853150044168077853)
XLA Ops:
  0.6 0.0 copy-start.1
  0.6 0.0 copy-start
  0.7 0.0 copy-start.5
  0.7 0.0 copy-start.6
  0.7 0.0 copy-start.4
  0.7 0.0 copy-start.3
  0.7 0.0 copy-start.2
  0.7 14.0 %prompt_states.1 = bf16[16,64,128]{2,1,0:T(8,128)(2,1)S(1)} custom-call(bf16[2048,4096]{1,0:T(8,128)(2,1)} %bitcast.19, bf16[4096,128]{1,0:T(8,128)(2,1)} %wk_hbm.1, bf16[4096,256]{1,0:T(8,128)(2,1)} %wv_hbm.1, bf16[2,4096]{1,0:T(2,128)(2,1)} %bitcast.20, bf16[2,4096]{1,0:T(2,128)(2,1)} %bitcast.21, f32[1,2]{1,0:T(1,128)} %bitcast.23, ...), custom_call_target="tpu_custom_call" | custom-call | tf_op jit(solution)/shard_map/prompt_states/pallas_call | solution.py:197
  14.7 15.8 %all_to_all.10.parts_ref = bf16[16,64,128]{2,1,0:T(8,128)(2,1)S(1)} all-to-all(bf16[16,64,128]{2,1,0:T(8,128)(2,1)S(1)} %prompt_states.1), channel_id=1, replica_groups=mesh['sp_0'=4,'sp_1'=4,'tp_0'=4,'tp_1'=2] {'sp_0','sp_1'}, dimensions={0} | all-to-all | bytes 524288 | tf_op jit(solution)/shard_map/all_to_all | solution.py:384
  30.5 0.0 copy-done.1
  30.5 0.0 copy-done
  30.5 0.0 copy-done.5
  30.5 0.0 copy-done.6
  30.5 0.0 copy-done.4
  30.5 0.0 copy-done.3
  30.5 0.0 copy-done.2
  30.5 1.9 %first_read.1 = (bf16[4,2,8,64]{3,2,1,0:T(8,128)(2,1)}, bf16[4,2,4]{2,1,0:T(2,128)(2,1)}, f32[2,4]{1,0:T(2,128)}, f32[128,128]{1,0:T(8,128)S(1)}) custom-call(f32[2,4]{1,0:T(2,128)S(1)} %bitcast.17, f32[2,4]{1,0:T(2,128)S(1)} %bitcast.18, bf16[16,64,128]{2,1,0:T(8,128)(2,1)S(1)} %all_to_all.10.parts_ref, bf16[3,128]{1,0:T(4,128)(2,1)S(1)} %copy-done.1, ...), custom_call_target="tpu_custom_call" | custom-call | tf_op jit(solution)/shard_map/first_read/pallas_call | solution.py:341
  32.4 16.8 %all_to_all.11 = f32[128,1,128]{2,1,0:T(1,128)S(1)} all-to-all(f32[128,1,128]{2,1,0:T(1,128)S(1)} %bitcast.16), channel_id=1, replica_groups=mesh['sp_0'=4,'sp_1'=4,'tp_0'=4,'tp_1'=2] {'sp_0','sp_1','tp_0','tp_1'}, dimensions={0} | all-to-all | bytes 131072 | tf_op jit(solution)/shard_map/all_to_all | solution.py:389
  49.2 0.7 %sum_parts.1 = bf16[4,32]{1,0:T(4,128)(2,1)} custom-call(f32[128,128]{1,0:T(8,128)S(1)} %bitcast.14), custom_call_target="tpu_custom_call" | custom-call | tf_op jit(solution)/shard_map/sum_parts/pallas_call | solution.py:365
Async XLA Ops:
  0.6 29.8 %copy-start.1 = (bf16[3,128]{1,0:T(4,128)(2,1)S(1)}, bf16[3,128]{1,0:T(4,128)(2,1)}, u32[]{:S(2)}) copy-start(bf16[3,128]{1,0:T(4,128)(2,1)} %taps_ref.1) | copy-start | bytes 2308
  0.6 29.8 %copy-start = (bf16[2,8,4096]{2,1,0:T(8,128)(2,1)S(1)}, bf16[2,8,4096]{2,1,0:T(8,128)(2,1)}, u32[]{:S(2)}) copy-start(bf16[2,8,4096]{2,1,0:T(8,128)(2,1)} %param.27) | copy-start | bytes 393220
  0.7 29.8 %copy-start.5 = (f32[4,2]{0,1:T(2,128)S(1)}, f32[4,2]{0,1:T(2,128)}, u32[]{:S(2)}) copy-start(f32[4,2]{0,1:T(2,128)} %param.26) | copy-start | bytes 100
  0.7 29.8 %copy-start.6 = (f32[4,2]{0,1:T(2,128)S(1)}, f32[4,2]{0,1:T(2,128)}, u32[]{:S(2)}) copy-start(f32[4,2]{0,1:T(2,128)} %param.25) | copy-start | bytes 100
  0.7 29.8 %copy-start.4 = (bf16[4,2,8]{2,1,0:T(2,128)(2,1)S(1)}, bf16[4,2,8]{2,1,0:T(2,128)(2,1)}, u32[]{:S(2)}) copy-start(bf16[4,2,8]{2,1,0:T(2,128)(2,1)} %value_ref.1) | copy-start | bytes 388
  0.7 29.8 %copy-start.3 = (bf16[4,2,64]{2,1,0:T(2,128)(2,1)S(1)}, bf16[4,2,64]{2,1,0:T(2,128)(2,1)}, u32[]{:S(2)}) copy-start(bf16[4,2,64]{2,1,0:T(2,128)(2,1)} %key_ref.1) | copy-start | bytes 3076
  0.7 29.8 %copy-start.2 = (bf16[4,2,64]{2,1,0:T(2,128)(2,1)S(1)}, bf16[4,2,64]{2,1,0:T(2,128)(2,1)}, u32[]{:S(2)}) copy-start(bf16[4,2,64]{2,1,0:T(2,128)(2,1)} %query_ref.1) | copy-start | bytes 3076
